TPU v7x, 32 devices: a whole 2x2x4 slice. The times are simulated.
32 devices in a mesh: sp: 4 (over z), fs: 4 (over y, x), tp: 2 (over core).
Axes of the slice: x: 2, y: 2, z: 4, core: 2. Of those that a mesh axis runs over, the one named last changes fastest.
Arguments:
- inputs: bfloat16 [16384, 2048], P(('fs', 'sp'), 'tp'), parts along dimension 0, may hold values from -270 to 270
- mix_gain: float32 [2048], replicated, may hold values from 0.1 to 1.9
- w_query: bfloat16 [2048, 1024], P(None, 'tp'), may hold values from -0.125 to 0.125
- w_key: bfloat16 [2048, 256], P(None, 'tp'), may hold values from -0.125 to 0.125
- w_value: bfloat16 [2048, 256], P(None, 'tp'), may hold values from -0.125 to 0.125
- query_gain: float32 [64], replicated, may hold values from 0 to 14, as said below
- key_gain: float32 [64], replicated, may hold values from 0 to 14, as said below
- sink_logit: float32 [16], P('tp'), may hold values from 3 to 7
- w_inner: bfloat16 [2048, 1024], P(None, 'tp'), may hold values from -0.125 to 0.125
- w_bmat: bfloat16 [2048, 512], P(None, 'tp'), may hold values from -0.125 to 0.125
- w_cmat: bfloat16 [2048, 512], P(None, 'tp'), may hold values from -0.125 to 0.125
- w_gate: bfloat16 [2048, 1024], P(None, 'tp'), may hold values from -0.125 to 0.125
- w_step: bfloat16 [2048, 2, 16], P(None, None, 'tp'), may hold values from -0.125 to 0.125
- conv_inner: bfloat16 [5, 1024], P(None, 'tp'), may hold values from -2.5 to 2.5
- conv_bmat: bfloat16 [5, 512], P(None, 'tp'), may hold values from -2.5 to 2.5
- conv_cmat: bfloat16 [5, 512], P(None, 'tp'), may hold values from -2.5 to 2.5
- step_bias: float32 [2, 16], P(None, 'tp'), may hold values from -1 to 1
- decay_rate: float32 [2, 16], P(None, 'tp'), may hold values from 0 to 1, as said below
- decay_offset: float32 [4096, 2, 16], P('sp', None, 'tp'), may hold values from -3 to 0, as said below
- start_state: float32 [8, 16, 64, 128], P('fs', 'tp'), parts along dimension 0, may hold values from -96 to 96
- group_gain: float32 [1024], P('tp'), may hold values from 0.1 to 1.9
- w_out_attn: bfloat16 [1024, 2048], P('tp'), may hold values from -1.5 to 1.5
- w_out_state: bfloat16 [1024, 2048], P('tp'), may hold values from -0.1875 to 0.1875
Outputs:
- mixed: bfloat16 [16384, 2048], P(('fs', 'sp', 'tp')), parts along dimension 0
There are 4 independent parts, one for each index of `fs`. A program takes and returns all parts, laid end to end along the dimension named above; an argument that names none is the same for every part. Nothing has to cross between parts.
Inputs may be any that keep to these rules, and one draw needn't show every extreme that they name: `query_gain`: positive. `key_gain`: positive. `decay_rate`: positive. `decay_offset`: never positive.
All inputs are finite; a program needn't handle non-finite values.
Results may differ from a plain program's by a relative error of at most 0.035.
Values may be sent and summed in bfloat16 or wider, within the bound.
A program may use at most 128 MiB of HBM per device.

v0:
```python
import functools

import jax
import jax.numpy as jnp
import numpy as np
from jax import lax
from jax.experimental import pallas as pl
from jax.experimental.pallas import tpu as pltpu
from jax.sharding import PartitionSpec as P

HEAD = 64
STATE = 128
CONV = 5
BLK = 128
LANE = 128
ROWS = 256
EDGE = 8

epsilon = 1e-06
rotary_base = 10000.0
F32 = jnp.float32
BF16 = jnp.bfloat16
MESH = pl.DeviceIdType.MESH


def mm(a, b):
    return jnp.dot(a, b, preferred_element_type=F32)


def mm_t(a, b):
    return lax.dot_general(a, b, (((1,), (1,)), ((), ())), preferred_element_type=F32)


def mm_hi(a, b):
    return jnp.dot(a, b, preferred_element_type=F32, precision=lax.Precision.HIGHEST)


def low_half(shape):
    return lax.broadcasted_iota(jnp.int32, shape, len(shape) - 1) < HEAD


def silu(v):
    return v / (1.0 + jnp.exp(-v))


def kernel(
    x_hbm, wq, wk, wv, wi, wb, wc, wg, ws, woa, wos,
    mix_gain, qgain1, kgain1, sink, taps_i, taps_b, taps_c, bias2, rate2, offs, start, ggain,
    cos_t, sin_t, cos_o, sin_o, expand,
    out_ref,
    w, wst, wo, xown, xpeer, xs, rs, kv, xbuf, qb, gb, st, cb, act, gs, dec, sb, z,
    psend, precv, kvlo, kvhi, xlo, xhi, chain_s, chain_r, sem_w, sem_x, sem_xs, sem_xr,
    sem_hs, sem_hr, sem_cs, sem_cr, sem_ps, sem_pr,
    *, n_sp,
):
    me = lax.axis_index("tp")
    idx = lax.axis_index("sp")
    peer = 1 - me
    T, half = x_hbm.shape
    nb = T // BLK
    nchunk = T // ROWS
    has_prev = idx > 0
    has_next = idx < n_sp - 1

    barrier = pltpu.get_barrier_semaphore()
    pl.semaphore_signal(barrier, inc=1, device_id={"tp": peer}, device_id_type=MESH)

    @pl.when(has_prev)
    def _():
        pl.semaphore_signal(barrier, inc=1, device_id={"sp": idx - 1}, device_id_type=MESH)

    @pl.when(has_next)
    def _():
        pl.semaphore_signal(barrier, inc=1, device_id={"sp": idx + 1}, device_id_type=MESH)

    own_copies = []
    for i in range(nchunk):
        c = pltpu.make_async_copy(
            x_hbm.at[pl.ds(i * ROWS, ROWS)], xown.at[pl.ds(i * ROWS, ROWS)], sem_x.at[i]
        )
        c.start()
        own_copies.append(c)
    wcopies = []
    col = 0
    for j, src in enumerate((wk, wv, wi, wb, wc, wq, wg, ws)):
        width = src.shape[1]
        dst = w.at[:, pl.ds(col, width)] if src is not ws else wst
        c = pltpu.make_async_copy(src, dst, sem_w.at[j])
        c.start()
        wcopies.append(c)
        col += width
    n_w = len(wcopies)
    na = woa.shape[0]
    oc = [
        pltpu.make_async_copy(woa, wo.at[pl.ds(0, na)], sem_w.at[n_w]),
        pltpu.make_async_copy(wos, wo.at[pl.ds(na, wos.shape[0])], sem_w.at[n_w + 1]),
    ]
    for c in oc:
        c.start()

    st[...] = jnp.zeros_like(st)
    cb[...] = jnp.zeros_like(cb)
    qgain = jnp.concatenate([qgain1[...]] * (LANE // HEAD), axis=1)
    kgain = jnp.concatenate([kgain1[...]] * (LANE // HEAD), axis=1)
    bias = jnp.concatenate([bias2[0:1, :], bias2[1:2, :]], axis=1)
    rate = jnp.concatenate([rate2[0:1, :], rate2[1:2, :]], axis=1)

    @pl.when(has_prev & has_next)
    def _():
        pl.semaphore_wait(barrier, 3)

    @pl.when(jnp.logical_not(has_prev & has_next))
    def _():
        pl.semaphore_wait(barrier, 2 if n_sp > 1 else 1)

    gath = []
    for i in range(nchunk):
        c = pltpu.make_async_remote_copy(
            src_ref=x_hbm.at[pl.ds(i * ROWS, ROWS)],
            dst_ref=xpeer.at[pl.ds(i * ROWS, ROWS)],
            send_sem=sem_xs.at[i],
            recv_sem=sem_xr.at[i],
            device_id={"tp": peer},
            device_id_type=MESH,
        )
        c.start()
        gath.append(c)

    gain_own = mix_gain[:, pl.ds(pl.multiple_of(me * half, LANE), half)]
    gain_peer = mix_gain[:, pl.ds(pl.multiple_of(peer * half, LANE), half)]
    for i in range(nchunk):
        own_copies[i].wait()
        gath[i].wait()

        def scale_rows(r, carry):
            rows = pl.ds(pl.multiple_of(i * ROWS + r * 32, 32), 32)
            a = xown[rows, :].astype(F32)
            b = xpeer[rows, :].astype(F32)
            total = jnp.sum(a * a + b * b, axis=1, keepdims=True)
            rs[rows, :] = jnp.broadcast_to(
                lax.rsqrt(total * (1.0 / (2 * half)) + epsilon), (32, LANE)
            )
            xs[rows, pl.ds(pl.multiple_of(me * half, LANE), half)] = (a * gain_own).astype(BF16)
            xs[rows, pl.ds(pl.multiple_of(peer * half, LANE), half)] = (b * gain_peer).astype(BF16)
            return carry

        lax.fori_loop(0, ROWS // 32, scale_rows, 0)

    co = cos_o[pl.ds(idx, 1), :]
    so = sin_o[pl.ds(idx, 1), :]

    def norm_rotate(v, gain, rows):
        shape = v.shape
        low = low_half(shape)
        sq = v * v
        s_lo = jnp.sum(jnp.where(low, sq, 0.0), axis=1, keepdims=True)
        s_hi = jnp.sum(jnp.where(low, 0.0, sq), axis=1, keepdims=True)
        v = v * lax.rsqrt(jnp.where(low, s_lo, s_hi) * (1.0 / HEAD) + epsilon) * gain
        ct = cos_t[rows, :]
        sn = sin_t[rows, :]
        cosine = co * ct - so * sn
        sine = so * ct + co * sn
        first = (lax.broadcasted_iota(jnp.int32, shape, 1) % HEAD) < HEAD // 2
        partner = jnp.where(first, -pltpu.roll(v, LANE - HEAD // 2, 1), pltpu.roll(v, HEAD // 2, 1))
        return v * cosine + partner * sine

    def row_chunk(i):
        start_row = pl.multiple_of(i * ROWS, ROWS)
        return start_row, pl.ds(start_row, ROWS)

    kvw = wk.shape[1]
    wcopies[0].wait()
    wcopies[1].wait()

    def kv_step(i, carry):
        r0, rows = row_chunk(i)
        p = mm(xs[rows, :], w[:, : 2 * kvw])
        scale = rs[rows, :]
        k = (p[:, :LANE] * scale).astype(BF16).astype(F32)
        v = (p[:, LANE:] * scale).astype(BF16).astype(F32)
        k = norm_rotate(k, kgain, rows)
        low = low_half(k.shape)
        k_sw = pltpu.roll(k, HEAD, 1)
        v_sw = pltpu.roll(v, HEAD, 1)
        dst = pl.ds(pl.multiple_of(r0 + BLK, BLK), ROWS)
        kv[dst, 0:LANE] = jnp.where(low, k, k_sw).astype(BF16)
        kv[dst, LANE : 2 * LANE] = jnp.where(low, k_sw, k).astype(BF16)
        kv[dst, 2 * LANE : 3 * LANE] = jnp.where(low, v, v_sw).astype(BF16)
        kv[dst, 3 * LANE : 4 * LANE] = jnp.where(low, v_sw, v).astype(BF16)
        return carry

    lax.fori_loop(0, nchunk, kv_step, 0)

    def remote(src, dst, ss, rsem, target):
        return pltpu.make_async_remote_copy(
            src_ref=src, dst_ref=dst, send_sem=ss, recv_sem=rsem,
            device_id={"sp": target}, device_id_type=MESH,
        )

    inner_w = wi.shape[1]
    state_w = wb.shape[1]
    xw = inner_w + 2 * state_w
    for j in (2, 3, 4):
        wcopies[j].wait()

    def x_step(i, carry):
        r0, rows = row_chunk(i)
        scale = rs[rows, :]
        dst = pl.ds(pl.multiple_of(r0 + EDGE, EDGE), ROWS)
        for s in range(0, xw, 256):
            p = mm(xs[rows, :], w[:, 2 * kvw + s : 2 * kvw + s + 256])
            for t in range(0, 256, LANE):
                xbuf[dst, s + t : s + t + LANE] = (p[:, t : t + LANE] * scale).astype(BF16).astype(F32)
        return carry

    kv_up = remote(kv.at[pl.ds(T, BLK)], kvlo, sem_hs.at[0], sem_hr.at[0], idx + 1)
    kv_dn = remote(kv.at[pl.ds(BLK, BLK)], kvhi, sem_hs.at[1], sem_hr.at[1], idx - 1)
    x_up = remote(xbuf.at[pl.ds(T, EDGE)], xlo, sem_hs.at[2], sem_hr.at[2], idx + 1)
    x_dn = remote(xbuf.at[pl.ds(EDGE, EDGE)], xhi, sem_hs.at[3], sem_hr.at[3], idx - 1)

    x_step(0, 0)

    @pl.when(has_next)
    def _():
        kv_up.start()

    @pl.when(has_prev)
    def _():
        kv_dn.start()

    lax.fori_loop(1, nchunk, x_step, 0)

    for j in (5, 6, 7):
        wcopies[j].wait()
    qcol = 2 * kvw + xw
    qw = wq.shape[1]
    gw = wg.shape[1]

    def q_step(i, carry):
        r0, rows = row_chunk(i)
        scale = rs[rows, :]
        xr = xs[rows, :]
        for s in range(0, qw, 256):
            p = mm(xr, w[:, qcol + s : qcol + s + 256])
            for t in range(0, 256, LANE):
                q = (p[:, t : t + LANE] * scale).astype(BF16).astype(F32)
                q = norm_rotate(q, qgain, rows).astype(BF16).astype(F32)
                qb[rows, s + t : s + t + LANE] = (q * HEAD ** (-0.5)).astype(BF16)
        for s in range(0, gw, 256):
            p = mm(xr, w[:, qcol + qw + s : qcol + qw + s + 256])
            for t in range(0, 256, LANE):
                gb[rows, s + t : s + t + LANE] = (p[:, t : t + LANE] * scale).astype(BF16)
        p = mm(xr, wst[...]) * scale[:, : wst.shape[1]] + bias
        step = jnp.maximum(p, 0.0) + jnp.log1p(jnp.exp(-jnp.abs(p)))
        st[rows, : wst.shape[1]] = step
        cb[rows, : wst.shape[1]] = -rate * step + offs[rows, :]
        return carry

    q_step(0, 0)

    @pl.when(has_next)
    def _():
        x_up.start()

    @pl.when(has_prev)
    def _():
        x_dn.start()

    lax.fori_loop(1, nchunk, q_step, 0)

    @pl.when(has_next)
    def _():
        kv_up.wait_send()
        x_up.wait_send()
        kv_dn.wait_recv()
        x_dn.wait_recv()
        kv[pl.ds(T + BLK, BLK), :] = kvhi[...]
        xbuf[pl.ds(T + EDGE, EDGE), :] = xhi[...]

    @pl.when(jnp.logical_not(has_next))
    def _():
        kv[pl.ds(T + BLK, BLK), :] = jnp.zeros((BLK, kv.shape[1]), BF16)
        xbuf[pl.ds(T + EDGE, EDGE), :] = jnp.zeros((EDGE, xw), F32)

    @pl.when(has_prev)
    def _():
        kv_dn.wait_send()
        x_dn.wait_send()
        kv_up.wait_recv()
        x_up.wait_recv()
        kv[pl.ds(0, BLK), :] = kvlo[...]
        xbuf[pl.ds(0, EDGE), :] = xlo[...]

    @pl.when(jnp.logical_not(has_prev))
    def _():
        kv[pl.ds(0, BLK), :] = jnp.zeros((BLK, kv.shape[1]), BF16)
        xbuf[pl.ds(0, EDGE), :] = jnp.zeros((EDGE, xw), F32)

    sq = (BLK, BLK)
    ri = lax.broadcasted_iota(jnp.int32, sq, 0)
    ci = lax.broadcasted_iota(jnp.int32, sq, 1)
    heads = inner_w // HEAD
    groups = state_w // STATE
    per_group = heads // groups
    gwid = per_group * HEAD
    low = low_half(sq)

    def spread(values, column):
        return jnp.broadcast_to(values[:, column : column + 1], sq)

    def paired(values, tile, direction):
        base = direction * heads + 2 * tile
        return jnp.where(low, spread(values, base), spread(values, base + 1))

    def state_step(b, carry):
        rows = pl.ds(pl.multiple_of(b * BLK, BLK), BLK)
        lower = jnp.where(ri >= ci, 1.0, 0.0).astype(F32)
        upper = jnp.where(ri <= ci, 1.0, 0.0).astype(F32)
        d = cb[rows, :]
        c = jnp.where(ci < heads, mm_hi(lower, d), mm_hi(upper, d))
        cb[rows, :] = c
        last = jnp.where(ci[:1] < heads, c[BLK - 1 : BLK, :], c[0:1, :])
        last8 = jnp.broadcast_to(last, (8, BLK))
        wide = jnp.exp(mm_hi(last8, expand[...]))
        dec[b, 0] = wide[:, :inner_w]
        dec[b, 1] = wide[:, inner_w:]
        load = st[rows, :] * jnp.exp(last - c)
        bt = []
        for s in range(xw - LANE, -1, -LANE):
            if s < inner_w:
                tap = taps_i[:, s : s + LANE].astype(F32)
            elif s < inner_w + state_w:
                tap = taps_b[:, s - inner_w : s - inner_w + LANE].astype(F32)
            else:
                o = s - inner_w - state_w
                tap = taps_c[:, o : o + LANE].astype(F32)
            win = xbuf[pl.ds(pl.multiple_of(b * BLK, BLK), BLK + 2 * EDGE), s : s + LANE]
            acc = jnp.zeros(sq, F32)
            for j in range(CONV):
                o = EDGE - CONV // 2 + j
                acc = acc + win[o : o + BLK] * tap[j : j + 1]
            a = silu(acc).astype(BF16)
            act[rows, s : s + LANE] = a
            if inner_w <= s < inner_w + state_w:
                bt.insert(0, a.astype(F32).T.astype(BF16))
            if s < inner_w:
                tile = s // LANE
                g = s // gwid
                af = a.astype(F32)
                for direction in range(2):
                    loaded = (af * paired(load, tile, direction)).astype(BF16)
                    gs[b, direction, :, s : s + LANE] = mm(bt[g], loaded)
        return carry

    lax.fori_loop(0, nb, state_step, 0)

    up = remote(chain_s.at[0], chain_r.at[0], sem_cs.at[0], sem_cr.at[0], idx + 1)
    dn = remote(chain_s.at[1], chain_r.at[1], sem_cs.at[1], sem_cr.at[1], idx - 1)

    def hop(direction, copy, first, has_source, has_target):
        @pl.when(has_source)
        def _():
            copy.wait_recv()

        @pl.when(has_target)
        def _():
            order = list(range(nb)) if direction == 0 else list(range(nb - 1, -1, -1))
            for s in range(0, inner_w, LANE):
                cols = slice(s, s + LANE)
                enter = jnp.where(
                    has_source, chain_r[direction, :, cols].astype(F32), start[direction, cols, :].T
                )
                total = enter
                for b in order:
                    total = total * dec[b, direction, 0:1, cols] + gs[b, direction, :, cols]
                chain_s[direction, :, cols] = total.astype(BF16)

    key_w = 3 * BLK
    aj = lax.broadcasted_iota(jnp.int32, (BLK, key_w), 1)
    ai = lax.broadcasted_iota(jnp.int32, (BLK, key_w), 0)
    reach = 2 * BLK
    kv_heads = kvw // HEAD
    q_per = (qw // HEAD) // kv_heads
    ones = jnp.ones((key_w, LANE), BF16)
    turn_up = (idx * nb) // n_sp
    turn_dn = ((n_sp - 1 - idx) * nb) // n_sp

    def attend(b, carry):
        @pl.when(b == turn_up)
        def _():
            hop(0, up, idx == 0, has_prev, has_next)

        @pl.when(b == turn_dn)
        def _():
            hop(1, dn, idx == n_sp - 1, has_next, has_prev)

        rows = pl.ds(pl.multiple_of(b * BLK, BLK), BLK)
        span = pl.ds(pl.multiple_of(b * BLK, BLK), key_w)
        lo = jnp.where((idx == 0) & (b == 0), BLK, 0)
        hi = jnp.where((idx == n_sp - 1) & (b == nb - 1), 2 * BLK - 1, key_w)
        valid = (aj >= jnp.maximum(ai, lo)) & (aj <= jnp.minimum(ai + reach, hi))
        for g in range(kv_heads):
            parts = []
            for t in range(q_per // 2):
                tile = g * (q_per // 2) + t
                q = qb[rows, tile * LANE : (tile + 1) * LANE]
                zero = jnp.zeros_like(q)
                parts += [jnp.where(low, q, zero), jnp.where(low, zero, q)]
            keys = kv[span, g * LANE : (g + 1) * LANE]
            vals = kv[span, (kv_heads + g) * LANE : (kv_heads + g + 1) * LANE]
            ext = jnp.concatenate([vals, ones], axis=1)
            s_all = mm_t(jnp.concatenate(parts, axis=0), keys)
            outs = []
            for r in range(q_per):
                s = jnp.where(valid, s_all[r * BLK : (r + 1) * BLK], -1e30)
                sk = sink[:, g * q_per + r : g * q_per + r + 1]
                m = jnp.maximum(jnp.max(s, axis=1, keepdims=True), sk)
                p = jnp.exp(s - m).astype(BF16)
                o = mm(p, ext)
                den = o[:, LANE:] + jnp.exp(sk - m)
                outs.append(o[:, :LANE] / den)
            for t in range(q_per // 2):
                tile = g * (q_per // 2) + t
                z[rows, tile * LANE : (tile + 1) * LANE] = jnp.where(
                    low, outs[2 * t], outs[2 * t + 1]
                ).astype(BF16)

        @pl.when((b == turn_up) & has_next)
        def _():
            up.start()

        @pl.when((b == turn_dn) & has_prev)
        def _():
            dn.start()

        return carry

    lax.fori_loop(0, nb, attend, 0)

    @pl.when(has_next)
    def _():
        up.wait_send()

    @pl.when(has_prev)
    def _():
        dn.wait_send()

    for direction in range(2):
        source = has_prev if direction == 0 else has_next
        order = list(range(nb)) if direction == 0 else list(range(nb - 1, -1, -1))
        for s in range(0, inner_w, LANE):
            cols = slice(s, s + LANE)
            total = jnp.where(
                source, chain_r[direction, :, cols].astype(F32), start[direction, cols, :].T
            )
            for b in order:
                sb[b, direction, :, cols] = total.astype(BF16)
                if b != order[-1]:
                    total = total * dec[b, direction, 0:1, cols] + gs[b, direction, :, cols]

    attn_w = qw

    def mix_block(b):
        rows = pl.ds(pl.multiple_of(b * BLK, BLK), BLK)
        c = cb[rows, :]
        step = st[rows, :]
        c_t = c.T
        step_t = step.T
        diag = ri == ci
        below = ri >= ci
        for g in range(groups):
            bm = act[rows, inner_w + g * STATE : inner_w + (g + 1) * STATE]
            cm = act[rows, inner_w + state_w + g * STATE : inner_w + state_w + (g + 1) * STATE]
            scores = mm_t(cm, bm)
            carried = [mm(cm, sb[b, d, :, g * gwid : (g + 1) * gwid]) for d in range(2)]
            gated = []
            for t in range(per_group // 2):
                tile = g * (per_group // 2) + t
                ws_ = []
                cols_f, cols_b = [], []
                for u in range(2):
                    h = 2 * tile + u
                    cf = spread(c, h)
                    cr = spread(c, heads + h)
                    cols_f.append(cf)
                    cols_b.append(cr)
                    arg = jnp.where(
                        below, cf - c_t[h : h + 1, :], cr - c_t[heads + h : heads + h + 1, :]
                    )
                    sf = step_t[h : h + 1, :]
                    sr = step_t[heads + h : heads + h + 1, :]
                    fac = jnp.where(diag, sf + sr, jnp.where(below, sf, sr))
                    ws_.append((scores * jnp.exp(arg) * fac).astype(BF16))
                y = mm(jnp.concatenate(ws_, axis=0), act[rows, tile * LANE : (tile + 1) * LANE])
                y = jnp.where(low, y[:BLK], y[BLK:])
                seg = slice(t * LANE, (t + 1) * LANE)
                y = y + carried[0][:, seg] * jnp.exp(jnp.where(low, cols_f[0], cols_f[1]))
                y = y + carried[1][:, seg] * jnp.exp(jnp.where(low, cols_b[0], cols_b[1]))
                gated.append(y * silu(gb[rows, tile * LANE : (tile + 1) * LANE].astype(F32)))
            total = sum(jnp.sum(v * v, axis=1, keepdims=True) for v in gated)
            inv = lax.rsqrt(total * (1.0 / gwid) + epsilon)
            for t, v in enumerate(gated):
                s = g * gwid + t * LANE
                z[rows, attn_w + s : attn_w + s + LANE] = (
                    v * inv * ggain[:, s : s + LANE]
                ).astype(BF16)

    for c in oc:
        c.wait()
    half_rows = T // 2
    steps = half_rows // ROWS
    width = wo.shape[1]

    def mix_rows(base):
        def one(k, carry):
            mix_block(base // BLK + k)
            return carry

        lax.fori_loop(0, ROWS // BLK, one, 0, unroll=True)

    copies = []
    for i in range(steps):
        base = peer * half_rows + i * ROWS
        mix_rows(base)
        zr = z[pl.ds(pl.multiple_of(base, ROWS), ROWS), :]
        for s in range(0, width, 512):
            psend[i * ROWS : (i + 1) * ROWS, s : s + 512] = mm(zr, wo[:, s : s + 512]).astype(BF16)
        copies.append(
            pltpu.make_async_remote_copy(
                src_ref=psend.at[pl.ds(i * ROWS, ROWS)],
                dst_ref=precv.at[pl.ds(i * ROWS, ROWS)],
                send_sem=sem_ps.at[i],
                recv_sem=sem_pr.at[i],
                device_id={"tp": peer},
                device_id_type=MESH,
            )
        )
        if i > 0:
            copies[i - 1].start()
    for i in range(steps):
        base = me * half_rows + i * ROWS
        mix_rows(base)
        if i == 0:
            copies[-1].start()
        zr = z[pl.ds(pl.multiple_of(base, ROWS), ROWS), :]
        for s in range(0, width, 512):
            part = mm(zr, wo[:, s : s + 512]).astype(BF16).astype(F32)
            if s == 0:
                copies[i].wait()
            got = precv[i * ROWS : (i + 1) * ROWS, s : s + 512].astype(F32)
            out_ref[i * ROWS : (i + 1) * ROWS, s : s + 512] = (part + got).astype(BF16)


def tables(tokens, count):
    lane = np.arange(LANE) % (HEAD // 2)
    frequency = rotary_base ** (-lane.astype(np.float64) / (HEAD // 2))
    inner = np.arange(tokens, dtype=np.float64)[:, None] * frequency[None, :]
    outer = np.arange(count, dtype=np.float64)[:, None] * tokens * frequency[None, :]
    return [f(a).astype(np.float32) for a in (inner, outer) for f in (np.cos, np.sin)]


def local(
    n_sp,
    inputs, mix_gain, w_query, w_key, w_value, query_gain, key_gain, sink_logit,
    w_inner, w_bmat, w_cmat, w_gate, w_step, conv_inner, conv_bmat, conv_cmat,
    step_bias, decay_rate, decay_offset, start_state, group_gain, w_out_attn, w_out_state,
):
    T, half = inputs.shape
    depth = w_query.shape[0]
    heads = w_step.shape[2]
    inner_w = w_inner.shape[1]
    state_w = w_bmat.shape[1]
    xw = inner_w + 2 * state_w
    kvw = w_key.shape[1]
    qw = w_query.shape[1]
    gw = w_gate.shape[1]
    width = w_out_attn.shape[1]
    nb = T // BLK
    nchunk = T // ROWS

    ws = w_step.reshape(depth, -1)
    offs = decay_offset.reshape(T, -1)
    start = start_state.reshape(2, inner_w, STATE)
    ct, sn, co, so = tables(T, n_sp)
    expand = np.zeros((LANE, 2 * inner_w), np.float32)
    for c in range(2 * heads):
        expand[c, c * HEAD : (c + 1) * HEAD] = 1.0
    any_spec = pl.BlockSpec(memory_space=pl.ANY)
    vm = pl.BlockSpec(memory_space=pltpu.VMEM)
    wcols = 2 * kvw + xw + qw + gw
    V = pltpu.VMEM
    dma = pltpu.SemaphoreType.DMA
    steps = T // 2 // ROWS
    scratch = [
        V((depth, wcols), BF16), V((depth, 2 * heads), BF16),
        V((w_out_attn.shape[0] + w_out_state.shape[0], width), BF16),
        V((T, half), BF16), V((T, half), BF16), V((T, 2 * half), BF16), V((T, LANE), F32),
        V((T + 2 * BLK, 4 * LANE), BF16), V((T + 2 * EDGE, xw), F32),
        V((T, qw), BF16), V((T, gw), BF16), V((T, LANE), F32), V((T, LANE), F32),
        V((T, xw), BF16),
        V((nb, 2, STATE, inner_w), F32), V((nb, 2, 8, inner_w), F32),
        V((nb, 2, STATE, inner_w), BF16),
        V((T, qw + inner_w), BF16),
        V((T // 2, width), BF16), V((T // 2, width), BF16),
        V((BLK, 4 * LANE), BF16), V((BLK, 4 * LANE), BF16),
        V((EDGE, xw), F32), V((EDGE, xw), F32),
        V((2, STATE, inner_w), BF16), V((2, STATE, inner_w), BF16),
        dma((10,)), dma((nchunk,)), dma((nchunk,)), dma((nchunk,)),
        dma((4,)), dma((4,)), dma((2,)), dma((2,)), dma((steps,)), dma((steps,)),
    ]
    return pl.pallas_call(
        functools.partial(kernel, n_sp=n_sp),
        out_shape=jax.ShapeDtypeStruct((T // 2, width), BF16),
        in_specs=[any_spec] * 11 + [vm] * 17,
        out_specs=vm,
        scratch_shapes=scratch,
        compiler_params=pltpu.CompilerParams(
            collective_id=0, has_side_effects=True, vmem_limit_bytes=67043328
        ),
        name="mixer",
    )(
        inputs, w_query, w_key, w_value, w_inner, w_bmat, w_cmat, w_gate, ws,
        w_out_attn, w_out_state,
        mix_gain.reshape(1, -1), query_gain.reshape(1, -1), key_gain.reshape(1, -1),
        sink_logit.reshape(1, -1), conv_inner, conv_bmat, conv_cmat, step_bias, decay_rate,
        offs, start,
        group_gain.reshape(1, -1), jnp.asarray(ct), jnp.asarray(sn), jnp.asarray(co),
        jnp.asarray(so), jnp.asarray(expand),
    )


def solution(mesh):
    return jax.shard_map(
        functools.partial(local, mesh.shape["sp"]),
        mesh=mesh,
        in_specs=(
            P(("fs", "sp"), "tp"),
            P(),
            P(None, "tp"),
            P(None, "tp"),
            P(None, "tp"),
            P(),
            P(),
            P("tp"),
            P(None, "tp"),
            P(None, "tp"),
            P(None, "tp"),
            P(None, "tp"),
            P(None, None, "tp"),
            P(None, "tp"),
            P(None, "tp"),
            P(None, "tp"),
            P(None, "tp"),
            P(None, "tp"),
            P("sp", None, "tp"),
            P("fs", "tp", None, None),
            P("tp"),
            P("tp", None),
            P("tp", None),
        ),
        out_specs=P(("fs", "sp", "tp"), None),
        check_vma=False,
    )
```

profile of v0, /device:TPU:0, one launch (start us, length us, event | category | flops | bytes accessed | tf_op | source)
XLA Modules:
  0.0 76.2 jit_solution(9327177949304526175)
XLA Ops:
  0.0 1.8 %copy.31.ws = bf16[2048,16]{1,0:T(8,128)(2,1)} copy(bf16[2048,16]{0,1:T(8,128)(2,1)} %bitcast.9) | data formatting | bytes 131072 | tf_op jit(solution)/shard_map/reshape | solution.py:581
  1.8 1.8 %copy.32.offs = f32[1024,16]{1,0:T(8,128)} copy(f32[1024,16]{0,1:T(8,128)} %bitcast.10) | data formatting | bytes 131072 | tf_op jit(solution)/shard_map/reshape | solution.py:582
  3.7 69.3 %mixer.1 = bf16[512,2048]{1,0:T(8,128)(2,1)} custom-call(bf16[1024,1024]{1,0:T(8,128)(2,1)} %x_hbm.1, bf16[2048,512]{1,0:T(8,128)(2,1)} %wq.1, bf16[2048,128]{1,0:T(8,128)(2,1)} %wk.1, bf16[2048,128]{1,0:T(8,128)(2,1)} %wv.1, bf16[2048,512]{1,0:T(8,128)(2,1)} %wi.1, bf16[2048,256]{1,0:T(8,128)(2,1)} %wb.1, bf16[2048,256]{1,0:T(8,128)(2,1)} %wc.1, ...), custom_call_target="tpu_custom_call" | custom-call | tf_op jit(solution)/shard_map/mixer/pallas_call | solution.py:611
  73.0 3.2 %copy.34 = bf16[512,2048]{1,0:T(8,128)(2,1)} copy(bf16[512,2048]{1,0:T(8,128)(2,1)} %mixer.1) | data formatting | bytes 4194304
where the time goes:
time: 76.4 us; the launch traced here: 76.2 us
  Pallas kernels  69.3 us (91%)
  local copies, waits for them, and re-layouts  6.84 us (9%)
    pallas_call x1, Pallas kernels, local(): pl.pallas_call(functools.partial(kernel, n_sp=n_sp), out_shape=jax.ShapeD...  69.3 us
    unnamed x1, local copies, waits for them, and re-layouts  3.16 us
    reshape x1, local copies, waits for them, and re-layouts, local(): ws = w_step.reshape(depth, -1)  1.84 us
    reshape x1, local copies, waits for them, and re-layouts, local(): offs = decay_offset.reshape(T, -1)  1.84 us

commit v1 on v0

v1 whole, which is shorter than its diff:
```python
import functools

import jax
import jax.numpy as jnp
import numpy as np
from jax import lax
from jax.experimental import pallas as pl
from jax.experimental.pallas import tpu as pltpu
from jax.sharding import PartitionSpec as P

HEAD = 64
STATE = 128
CONV = 5
BLK = 128
LANE = 128
ROWS = 256
EDGE = 8

epsilon = 1e-06
rotary_base = 10000.0
LOG2E = 1.4426950408889634
NEG = -1e30
F32 = jnp.float32
BF16 = jnp.bfloat16
MESH = pl.DeviceIdType.MESH


def mm(a, b):
    return jnp.dot(a, b, preferred_element_type=F32)


def mm_t(a, b):
    return lax.dot_general(a, b, (((1,), (1,)), ((), ())), preferred_element_type=F32)


def silu(v):
    return v / (1.0 + jnp.exp(-v))


def rounded(v):
    return v.astype(BF16).astype(F32)


def column(row):
    return jnp.broadcast_to(row, (LANE, LANE)).T


def pad_row(row):
    return jnp.concatenate([row, jnp.zeros((1, LANE - row.shape[1]), F32)], axis=1)


def pieces(v):
    hi = v.astype(BF16)
    rest = v - hi.astype(F32)
    mid = rest.astype(BF16)
    lo = (rest - mid.astype(F32)).astype(BF16)
    return hi, mid, lo


def kernel(
    x_hbm, wq, wk, wv, wi, wb, wc, wg, woa, wos,
    ws, mix_gain, qgain1, kgain1, sink, taps_i, taps_b, taps_c, bias2, rate2, offs, start, ggain,
    cos_t, sin_t, cos_o, sin_o, tri,
    out_hbm,
    w, wsp, wo, xown, xpeer, xs, rs, rot, kn, vt, xb, qt, gt, bc, xt, st, ct, dec, ld, ggt, bias_m,
    gs, agg, dtot, sb, z, psend, precv, outv, xhalo, chain_s, chain_r,
    sem_w, sem_x, sem_xs, sem_xr, sem_hs, sem_hr, sem_cs, sem_cr, sem_ps, sem_pr, sem_o,
    *, n_sp,
):
    me = lax.axis_index("tp")
    idx = lax.axis_index("sp")
    peer = 1 - me
    T, half = x_hbm.shape
    nb = T // BLK
    nchunk = T // ROWS
    per = ROWS // BLK
    has_prev = idx > 0
    has_next = idx < n_sp - 1

    barrier = pltpu.get_barrier_semaphore()
    pl.semaphore_signal(barrier, inc=1, device_id={"tp": peer}, device_id_type=MESH)

    @pl.when(has_prev)
    def _():
        pl.semaphore_signal(barrier, inc=1, device_id={"sp": idx - 1}, device_id_type=MESH)

    @pl.when(has_next)
    def _():
        pl.semaphore_signal(barrier, inc=1, device_id={"sp": idx + 1}, device_id_type=MESH)

    own_copies = []
    for i in range(nchunk):
        c = pltpu.make_async_copy(
            x_hbm.at[pl.ds(i * ROWS, ROWS)], xown.at[pl.ds(i * ROWS, ROWS)], sem_x.at[i]
        )
        c.start()
        own_copies.append(c)
    wcopies = []
    col = 0
    for j, src in enumerate((wi, wb, wc, wk, wv, wq, wg)):
        width = src.shape[1]
        c = pltpu.make_async_copy(src, w.at[:, pl.ds(col, width)], sem_w.at[j])
        c.start()
        wcopies.append(c)
        col += width
    n_w = len(wcopies)
    na = woa.shape[0]
    oc = [
        pltpu.make_async_copy(woa, wo.at[pl.ds(0, na)], sem_w.at[n_w]),
        pltpu.make_async_copy(wos, wo.at[pl.ds(na, wos.shape[0])], sem_w.at[n_w + 1]),
    ]
    for c in oc:
        c.start()

    inner_w = wi.shape[1]
    state_w = wb.shape[1]
    xw = inner_w + 2 * state_w
    kvw = wk.shape[1]
    qw = wq.shape[1]
    gw = wg.shape[1]
    kvcol = xw
    qcol = xw + 2 * kvw
    gcol = qcol + qw
    hd2 = ws.shape[0]
    heads = hd2 // 2
    groups = state_w // STATE
    per_group = heads // groups
    gwid = per_group * HEAD
    kv_heads = kvw // HEAD
    q_per = (qw // HEAD) // kv_heads
    sq = (BLK, BLK)
    ri = lax.broadcasted_iota(jnp.int32, sq, 0)
    ci = lax.broadcasted_iota(jnp.int32, sq, 1)

    wsp[hd2:, :] = jnp.zeros((LANE - hd2, wsp.shape[1]), BF16)
    wsp[0:hd2, :] = ws[...]
    qt[...] = jnp.zeros_like(qt)
    agg[...] = jnp.zeros_like(agg)
    qg = column(pad_row(qgain1[...] * (HEAD ** (-0.5) * LOG2E)))
    kg = column(pad_row(kgain1[...]))
    hh = HEAD // 2
    co = cos_o[idx]
    so = sin_o[idx]
    for b in range(nb):
        cols = slice(b * BLK, (b + 1) * BLK)
        c0 = cos_t[:, cols]
        s0 = sin_t[:, cols]
        cosine = co * c0 - so * s0
        sine = so * c0 + co * s0
        for k, gain in enumerate((qg, kg)):
            ga, gb = gain[0:hh], gain[hh:HEAD]
            rot[k, b, 0:hh] = ga * cosine
            rot[k, b, hh : 2 * hh] = gb * sine
            rot[k, b, 2 * hh : 3 * hh] = gb * cosine
            rot[k, b, 3 * hh : 4 * hh] = ga * sine
    bias = column(pad_row(jnp.concatenate([bias2[0:1, :], bias2[1:2, :]], axis=1)))[0:hd2]
    rate = column(pad_row(jnp.concatenate([rate2[0:1, :], rate2[1:2, :]], axis=1)))[0:hd2]
    for s in range(0, inner_w, LANE):
        ggt[s : s + LANE, :] = column(ggain[:, s : s + LANE])
    bias_m[0] = jnp.where(ri >= ci, 0.0, NEG)
    bias_m[1] = jnp.where(ri <= ci, 0.0, NEG)

    @pl.when(has_prev & has_next)
    def _():
        pl.semaphore_wait(barrier, 3)

    @pl.when(jnp.logical_not(has_prev & has_next))
    def _():
        pl.semaphore_wait(barrier, 2 if n_sp > 1 else 1)

    gath = []
    for i in range(nchunk):
        c = pltpu.make_async_remote_copy(
            src_ref=x_hbm.at[pl.ds(i * ROWS, ROWS)],
            dst_ref=xpeer.at[pl.ds(i * ROWS, ROWS)],
            send_sem=sem_xs.at[i],
            recv_sem=sem_xr.at[i],
            device_id={"tp": peer},
            device_id_type=MESH,
        )
        c.start()
        gath.append(c)

    gain_own = mix_gain[:, pl.ds(pl.multiple_of(me * half, LANE), half)]
    gain_peer = mix_gain[:, pl.ds(pl.multiple_of(peer * half, LANE), half)]

    def scale_half(i, src, gain, base, add):
        dst = pl.multiple_of(base * half, LANE)

        def body(r, carry):
            rows = pl.ds(pl.multiple_of(i * ROWS + r * 32, 32), 32)
            total = rs[rows, :] if add else jnp.zeros((32, LANE), F32)
            for s in range(0, half, LANE):
                a = src[rows, s : s + LANE].astype(F32)
                total = total + a * a
                xs[rows, pl.ds(pl.multiple_of(dst + s, LANE), LANE)] = (
                    a * gain[:, s : s + LANE]
                ).astype(BF16)
            rs[rows, :] = total
            return carry

        lax.fori_loop(0, ROWS // 32, body, 0, unroll=2)

    def finish_scale(i):
        rows = slice(i * ROWS, (i + 1) * ROWS)
        total = jnp.sum(rs[rows, :], axis=1, keepdims=True)
        rs[rows, :] = jnp.broadcast_to(
            lax.rsqrt(total * (1.0 / (2 * half)) + epsilon), (ROWS, LANE)
        )

    for i in range(nchunk):
        own_copies[i].wait()
        scale_half(i, xown, gain_own, me, False)
    for i in range(nchunk):
        gath[i].wait()
        scale_half(i, xpeer, gain_peer, peer, True)
        finish_scale(i)

    def row_chunk(i):
        start_row = pl.multiple_of(i * ROWS, ROWS)
        return start_row, pl.ds(start_row, ROWS)

    def norm_rotate(v, k, b):
        inv = lax.rsqrt(jnp.sum(v * v, axis=0, keepdims=True) * (1.0 / HEAD) + epsilon)
        a, c = v[0:hh], v[hh:HEAD]
        first = (a * rot[k, b, 0:hh] - c * rot[k, b, hh : 2 * hh]) * inv
        second = (c * rot[k, b, 2 * hh : 3 * hh] + a * rot[k, b, 3 * hh : 4 * hh]) * inv
        return jnp.concatenate([first, second], axis=0)

    def remote(src, dst, ss, rsem, target):
        return pltpu.make_async_remote_copy(
            src_ref=src, dst_ref=dst, send_sem=ss, recv_sem=rsem,
            device_id={"sp": target}, device_id_type=MESH,
        )

    for j in (0, 1, 2):
        wcopies[j].wait()

    def x_step(i, carry):
        r0, rows = row_chunk(i)
        scale = rs[rows, :]
        xr = xs[rows, :]
        dst = pl.ds(pl.multiple_of(r0 + EDGE, EDGE), ROWS)
        for s in range(0, xw, 256):
            p = mm(xr, w[:, s : s + 256])
            for t in range(0, 256, LANE):
                xb[(s + t) // LANE, dst, :] = rounded(p[:, t : t + LANE] * scale)
        p = mm_t(xr, wsp[...]) * scale
        pt = p.T[0:hd2]
        for u in range(per):
            b = i * per + u
            v = pt[:, u * BLK : (u + 1) * BLK] + bias
            step = jnp.maximum(v, 0.0) + jnp.log1p(jnp.exp(-jnp.abs(v)))
            st[b] = step
            ld[b] = -rate * step + offs[:, pl.ds(pl.multiple_of(b * BLK, BLK), BLK)]
        return carry

    lax.fori_loop(0, nchunk, x_step, 0)

    x_up = remote(xb.at[:, pl.ds(T, EDGE)], xhalo.at[0], sem_hs.at[2], sem_hr.at[2], idx + 1)
    x_dn = remote(xb.at[:, pl.ds(EDGE, EDGE)], xhalo.at[1], sem_hs.at[3], sem_hr.at[3], idx - 1)
    k_up = remote(kn.at[pl.ds(T, BLK)], kn.at[pl.ds(0, BLK)], sem_hs.at[0], sem_hr.at[0], idx + 1)
    k_dn = remote(kn.at[pl.ds(BLK, BLK)], kn.at[pl.ds(T + BLK, BLK)], sem_hs.at[1], sem_hr.at[1], idx - 1)
    v_up = remote(vt.at[:, pl.ds(T, BLK)], vt.at[:, pl.ds(0, BLK)], sem_hs.at[4], sem_hr.at[4], idx + 1)
    v_dn = remote(vt.at[:, pl.ds(BLK, BLK)], vt.at[:, pl.ds(T + BLK, BLK)], sem_hs.at[5], sem_hr.at[5], idx - 1)

    @pl.when(has_next)
    def _():
        x_up.start()

    @pl.when(has_prev)
    def _():
        x_dn.start()

    wcopies[3].wait()
    wcopies[4].wait()

    def kv_step(i, carry):
        r0, rows = row_chunk(i)
        p = mm(xs[rows, :], w[:, kvcol : kvcol + 2 * kvw])
        scale = rs[rows, :]
        for u in range(per):
            b = i * per + u
            part = slice(u * BLK, (u + 1) * BLK)
            kt = rounded(p[part, :LANE] * scale[part]).T
            kt = jnp.concatenate(
                [norm_rotate(kt[h * HEAD : (h + 1) * HEAD], 1, b) for h in range(kv_heads)], axis=0
            )
            dst = pl.multiple_of(r0 + (u + 1) * BLK, BLK)
            kn[pl.ds(dst, BLK), :] = kt.T.astype(BF16)
            vt[:, pl.ds(dst, BLK)] = (p[part, LANE:] * scale[part]).T.astype(BF16)
        return carry

    lax.fori_loop(0, nchunk, kv_step, 0)

    @pl.when(has_next)
    def _():
        k_up.start()
        v_up.start()

    @pl.when(has_prev)
    def _():
        k_dn.start()
        v_dn.start()

    lhs = []
    for b in range(nb):
        lhs += list(pieces(ld[b]))
    sums = mm(jnp.concatenate(lhs, axis=0), tri[...])
    last_f = last_b = None
    for b in range(nb):
        tot = sums[3 * b * hd2 : (3 * b + 1) * hd2]
        tot = tot + sums[(3 * b + 1) * hd2 : (3 * b + 2) * hd2]
        tot = (tot + sums[(3 * b + 2) * hd2 : (3 * b + 3) * hd2]) * LOG2E
        c = jnp.concatenate([tot[0:heads, 0:BLK], tot[heads:, BLK:]], axis=0)
        ct[b] = c
        end = jnp.concatenate(
            [
                jnp.broadcast_to(c[0:heads, BLK - 1 : BLK], (heads, BLK)),
                jnp.broadcast_to(c[heads:, 0:1], (heads, BLK)),
            ],
            axis=0,
        )
        dec[b] = jnp.exp2(end)
        ld[b] = st[b] * jnp.exp2(end - c)
        total = end if b == 0 else total + end
        if b < nb - 1:
            dtot[1 + b] = jnp.exp2(total)
    dtot[0] = jnp.exp2(total)

    @pl.when(has_next)
    def _():
        x_up.wait_send()
        x_dn.wait_recv()
        xb[:, pl.ds(T + EDGE, EDGE), :] = xhalo[1]

    @pl.when(jnp.logical_not(has_next))
    def _():
        xb[:, pl.ds(T + EDGE, EDGE), :] = jnp.zeros((xb.shape[0], EDGE, LANE), F32)

    @pl.when(has_prev)
    def _():
        x_dn.wait_send()
        x_up.wait_recv()
        xb[:, pl.ds(0, EDGE), :] = xhalo[0]

    @pl.when(jnp.logical_not(has_prev))
    def _():
        xb[:, pl.ds(0, EDGE), :] = jnp.zeros((xb.shape[0], EDGE, LANE), F32)

    def spread(values, row, n):
        return jnp.broadcast_to(values[row : row + 1, :], (n, LANE))

    def state_step(b, carry):
        rows = pl.ds(pl.multiple_of(b * BLK, BLK), BLK)
        load = ld[b]
        before = jnp.where(b == 0, jnp.ones((hd2, LANE), F32), dtot[b])
        dc = dec[b]
        for tile in list(range(inner_w // LANE, xw // LANE)) + list(range(inner_w // LANE)):
            s = tile * LANE
            if s < inner_w:
                tap = taps_i[:, s : s + LANE].astype(F32)
            elif s < inner_w + state_w:
                tap = taps_b[:, s - inner_w : s - inner_w + LANE].astype(F32)
            else:
                o = s - inner_w - state_w
                tap = taps_c[:, o : o + LANE].astype(F32)
            acc = None
            for j in range(CONV):
                win = xb[tile, pl.ds(b * BLK + (EDGE - CONV // 2 + j), BLK), :]
                term = win * tap[j : j + 1]
                acc = term if acc is None else acc + term
            a = silu(acc)
            if s >= inner_w:
                bc[rows, s - inner_w : s - inner_w + LANE] = a.astype(BF16)
                continue
            at = rounded(a.T)
            xt[b, s : s + LANE, :] = at.astype(BF16)
            g = s // gwid
            bm = bc[rows, g * STATE : (g + 1) * STATE]
            loaded = []
            for direction in range(2):
                for u in range(LANE // HEAD):
                    h = tile * (LANE // HEAD) + u
                    loaded.append(
                        (at[u * HEAD : (u + 1) * HEAD] * spread(load, direction * heads + h, HEAD)).astype(BF16)
                    )
            gsum = mm(jnp.concatenate(loaded, axis=0), bm)
            for direction in range(2):
                part = gsum[direction * LANE : (direction + 1) * LANE]
                gs[b, direction, s : s + LANE, :] = part
                old = agg[direction, s : s + LANE, :]
                for u in range(LANE // HEAD):
                    h = tile * (LANE // HEAD) + u
                    sl = slice(u * HEAD, (u + 1) * HEAD)
                    if direction == 0:
                        new = old[sl] * spread(dc, h, HEAD) + part[sl]
                    else:
                        new = old[sl] + part[sl] * spread(before, heads + h, HEAD)
                    agg[direction, s + u * HEAD : s + (u + 1) * HEAD, :] = new
        return carry

    lax.fori_loop(0, nb, state_step, 0)

    hops = [
        [
            remote(
                chain_s.at[d, pl.ds(g * gwid, gwid)], chain_r.at[d, pl.ds(g * gwid, gwid)],
                sem_cs.at[d * groups + g], sem_cr.at[d * groups + g],
                idx + 1 if d == 0 else idx - 1,
            )
            for g in range(groups)
        ]
        for d in range(2)
    ]
    sources = (has_prev, has_next)
    targets = (has_next, has_prev)
    order_of = (idx, n_sp - 1 - idx)

    def hop(direction, inner):
        for g in range(groups):
            if inner:
                hops[direction][g].wait_recv()
            for u in range(per_group):
                h = g * per_group + u
                rows = slice(h * HEAD, (h + 1) * HEAD)
                enter = chain_r[direction, rows, :].astype(F32) if inner else start[direction, rows, :]
                out = enter * spread(dtot[0], direction * heads + h, HEAD) + agg[direction, rows, :]
                chain_s[direction, rows, :] = out.astype(BF16)
            hops[direction][g].start()

    for d in range(2):
        @pl.when(targets[d] & jnp.logical_not(sources[d]))
        def _(d=d):
            hop(d, False)

    slots = nchunk + nb

    def maybe_hop(slot):
        for d in range(2):
            turn = (order_of[d] * slots) // max(n_sp - 1, 1)

            @pl.when((slot == turn) & targets[d] & sources[d])
            def _(d=d):
                hop(d, True)

    wcopies[5].wait()
    wcopies[6].wait()

    def q_step(i, carry):
        maybe_hop(i)
        r0, rows = row_chunk(i)
        scale = rs[rows, :]
        xr = xs[rows, :]
        for s in range(0, qw, 256):
            p = mm(xr, w[:, qcol + s : qcol + s + 256])
            for u in range(per):
                b = i * per + u
                part = slice(u * BLK, (u + 1) * BLK)
                for t in range(0, 256, LANE):
                    q = rounded(p[part, t : t + LANE] * scale[part]).T
                    for v in range(LANE // HEAD):
                        h = (s + t) // HEAD + v
                        g = h // q_per
                        qt[b, g * HEAD : (g + 1) * HEAD, h * BLK : (h + 1) * BLK] = norm_rotate(
                            q[v * HEAD : (v + 1) * HEAD], 0, b
                        ).astype(BF16)
        for s in range(0, gw, 256):
            p = mm(xr, w[:, gcol + s : gcol + s + 256])
            for u in range(per):
                b = i * per + u
                part = slice(u * BLK, (u + 1) * BLK)
                for t in range(0, 256, LANE):
                    gate = rounded(p[part, t : t + LANE] * scale[part]).T
                    gt[b, s + t : s + t + LANE, :] = silu(gate)
        return carry

    lax.fori_loop(0, nchunk, q_step, 0)

    @pl.when(has_next)
    def _():
        k_up.wait_send()
        v_up.wait_send()
        k_dn.wait_recv()
        v_dn.wait_recv()

    @pl.when(jnp.logical_not(has_next))
    def _():
        kn[pl.ds(T + BLK, BLK), :] = jnp.zeros((BLK, kvw), BF16)
        vt[:, pl.ds(T + BLK, BLK)] = jnp.zeros((kvw, BLK), BF16)

    @pl.when(has_prev)
    def _():
        k_dn.wait_send()
        v_dn.wait_send()
        k_up.wait_recv()
        v_up.wait_recv()

    @pl.when(jnp.logical_not(has_prev))
    def _():
        kn[pl.ds(0, BLK), :] = jnp.zeros((BLK, kvw), BF16)
        vt[:, pl.ds(0, BLK)] = jnp.zeros((kvw, BLK), BF16)

    key_w = 3 * BLK
    ones = jnp.ones((16, key_w), BF16)
    sinks = sink[...] * LOG2E

    def attend(b, carry):
        maybe_hop(nchunk + b)
        rows = pl.ds(pl.multiple_of(b * BLK, BLK), BLK)
        span = pl.ds(pl.multiple_of(b * BLK, BLK), key_w)
        keys = kn[span, :]
        lo = bias_m[0] + jnp.where((idx == 0) & (b == 0), NEG, 0.0)
        hi = bias_m[1] + jnp.where((idx == n_sp - 1) & (b == nb - 1), NEG, 0.0)
        for pair in range(qw // HEAD // 2):
            g = 2 * pair // q_per
            vals = jnp.concatenate([vt[g * HEAD : (g + 1) * HEAD, span], ones], axis=0)
            s_all = mm(keys, qt[b, :, 2 * pair * BLK : 2 * (pair + 1) * BLK])
            probs, adds = [], []
            for u in range(2):
                h = 2 * pair + u
                s = s_all[:, u * BLK : (u + 1) * BLK]
                s = jnp.concatenate([s[0:BLK] + lo, s[BLK : 2 * BLK], s[2 * BLK :] + hi], axis=0)
                sk = jnp.broadcast_to(sinks[:, h : h + 1], (1, BLK))
                m = jnp.maximum(jnp.max(s, axis=0, keepdims=True), sk)
                probs.append(jnp.exp2(s - m).astype(BF16))
                adds.append(jnp.exp2(sk - m))
            o = mm(vals, jnp.concatenate(probs, axis=1))
            outs = []
            for u in range(2):
                cols = slice(u * BLK, (u + 1) * BLK)
                inv = 1.0 / (o[HEAD : HEAD + 1, cols] + adds[u])
                outs.append(o[0:HEAD, cols] * inv)
            z[rows, pair * LANE : (pair + 1) * LANE] = jnp.concatenate(outs, axis=0).T.astype(BF16)
        return carry

    lax.fori_loop(0, nb, attend, 0)

    for d in range(2):
        @pl.when(targets[d])
        def _(d=d):
            for c in hops[d]:
                c.wait_send()

        @pl.when(sources[d] & jnp.logical_not(targets[d]))
        def _(d=d):
            for c in hops[d]:
                c.wait_recv()

    for d in range(2):
        order = list(range(nb)) if d == 0 else list(range(nb - 1, -1, -1))
        for h in range(heads):
            rows = slice(h * HEAD, (h + 1) * HEAD)
            total = jnp.where(sources[d], chain_r[d, rows, :].astype(F32), start[d, rows, :])
            for b in order:
                sb[b, d, rows, :] = total.astype(BF16)
                if b != order[-1]:
                    total = total * spread(dec[b], d * heads + h, HEAD) + gs[b, d, rows, :]

    attn_w = qw
    zero_pad = jnp.zeros((LANE - hd2, LANE), F32)

    def mix_block(b):
        rows = pl.ds(pl.multiple_of(b * BLK, BLK), BLK)
        c = ct[b]
        step = st[b]
        e = c - jnp.log2(jnp.maximum(step, 1e-37))
        en = jnp.concatenate([e, zero_pad], axis=0).T
        both = jnp.log2(jnp.maximum(step[0:heads] + step[heads:], 1e-37))
        grow = jnp.exp2(c)
        before = ri < ci
        same = ri == ci
        for g in range(groups):
            bm = bc[rows, g * STATE : (g + 1) * STATE]
            cm = bc[rows, state_w + g * STATE : state_w + (g + 1) * STATE]
            scores = mm_t(bm, cm)
            states = jnp.concatenate(
                [sb[b, d, g * gwid : (g + 1) * gwid, :] for d in range(2)], axis=0
            )
            carried = mm_t(states, cm)
            gated = []
            for u in range(per_group):
                h = g * per_group + u
                arg = jnp.where(
                    before,
                    spread(c, h, BLK) - jnp.broadcast_to(en[:, h : h + 1], sq),
                    spread(c, heads + h, BLK) - jnp.broadcast_to(en[:, heads + h : heads + h + 1], sq),
                )
                arg = jnp.where(same, spread(both, h, BLK), arg)
                weights = (scores * jnp.exp2(arg)).astype(BF16)
                y = mm(xt[b, h * HEAD : (h + 1) * HEAD, :], weights)
                y = y + carried[u * HEAD : (u + 1) * HEAD] * spread(grow, h, HEAD)
                y = y + carried[gwid + u * HEAD : gwid + (u + 1) * HEAD] * spread(grow, heads + h, HEAD)
                gated.append(y * gt[b, h * HEAD : (h + 1) * HEAD, :])
            total = sum(jnp.sum(v * v, axis=0, keepdims=True) for v in gated)
            inv = lax.rsqrt(total * (1.0 / gwid) + epsilon)
            for t in range(per_group // 2):
                s = g * gwid + t * LANE
                v = jnp.concatenate([gated[2 * t], gated[2 * t + 1]], axis=0)
                z[rows, attn_w + s : attn_w + s + LANE] = (v * inv * ggt[s : s + LANE, :]).T.astype(BF16)

    for c in oc:
        c.wait()
    half_rows = T // 2
    steps = half_rows // ROWS
    width = wo.shape[1]

    def mix_rows(base):
        def one(k, carry):
            mix_block(base // BLK + k)
            return carry

        lax.fori_loop(0, ROWS // BLK, one, 0, unroll=True)

    copies = [
        pltpu.make_async_remote_copy(
            src_ref=psend.at[pl.ds(i * ROWS, ROWS)],
            dst_ref=precv.at[pl.ds(i * ROWS, ROWS)],
            send_sem=sem_ps.at[i],
            recv_sem=sem_pr.at[i],
            device_id={"tp": peer},
            device_id_type=MESH,
        )
        for i in range(steps)
    ]
    outs = [
        pltpu.make_async_copy(
            outv.at[pl.ds(i * ROWS, ROWS)], out_hbm.at[pl.ds(i * ROWS, ROWS)], sem_o.at[i]
        )
        for i in range(steps)
    ]
    for i in range(steps):
        base = peer * half_rows + i * ROWS
        mix_rows(base)
        zr = z[pl.ds(pl.multiple_of(base, ROWS), ROWS), :]
        for s in range(0, width, 512):
            psend[i * ROWS : (i + 1) * ROWS, s : s + 512] = mm(zr, wo[:, s : s + 512]).astype(BF16)
        copies[i].start()
    for i in range(steps):
        base = me * half_rows + i * ROWS
        mix_rows(base)
        zr = z[pl.ds(pl.multiple_of(base, ROWS), ROWS), :]
        for s in range(0, width, 512):
            part = rounded(mm(zr, wo[:, s : s + 512]))
            if s == 0:
                copies[i].wait()
            got = precv[i * ROWS : (i + 1) * ROWS, s : s + 512].astype(F32)
            outv[i * ROWS : (i + 1) * ROWS, s : s + 512] = (part + got).astype(BF16)
        outs[i].start()
    for c in outs:
        c.wait()


def tables(tokens, count):
    half = HEAD // 2
    frequency = rotary_base ** (-np.arange(half, dtype=np.float64) / half)
    inner = frequency[:, None] * np.arange(tokens, dtype=np.float64)[None, :]
    outer = np.arange(count, dtype=np.float64)[:, None] * tokens * frequency[None, :]
    outer = np.broadcast_to(outer[:, :, None], (count, half, LANE))
    return [f(a).astype(np.float32) for a in (inner, outer) for f in (np.cos, np.sin)]


def local(
    n_sp,
    inputs, mix_gain, w_query, w_key, w_value, query_gain, key_gain, sink_logit,
    w_inner, w_bmat, w_cmat, w_gate, w_step, conv_inner, conv_bmat, conv_cmat,
    step_bias, decay_rate, decay_offset, start_state, group_gain, w_out_attn, w_out_state,
):
    T, half = inputs.shape
    depth = w_query.shape[0]
    heads = w_step.shape[2]
    inner_w = w_inner.shape[1]
    state_w = w_bmat.shape[1]
    xw = inner_w + 2 * state_w
    kvw = w_key.shape[1]
    qw = w_query.shape[1]
    gw = w_gate.shape[1]
    width = w_out_attn.shape[1]
    nb = T // BLK
    nchunk = T // ROWS
    groups = state_w // STATE

    ws = jnp.transpose(w_step, (1, 2, 0)).reshape(2 * heads, depth)
    offs = jnp.transpose(decay_offset, (1, 2, 0)).reshape(2 * heads, T)
    start = start_state.reshape(2, inner_w, STATE)
    ct, sn, co, so = tables(T, n_sp)
    tri = np.triu(np.ones((BLK, BLK), np.float32))
    tri = np.concatenate([tri, tri.T], axis=1)
    any_spec = pl.BlockSpec(memory_space=pl.ANY)
    vm = pl.BlockSpec(memory_space=pltpu.VMEM)
    wcols = 2 * kvw + xw + qw + gw
    V = pltpu.VMEM
    dma = pltpu.SemaphoreType.DMA
    steps = T // 2 // ROWS
    hd2 = 2 * heads
    scratch = [
        V((depth, wcols), BF16), V((LANE, depth), BF16),
        V((w_out_attn.shape[0] + w_out_state.shape[0], width), BF16),
        V((T, half), BF16), V((T, half), BF16), V((T, 2 * half), BF16), V((T, LANE), F32),
        V((2, nb, 2 * HEAD, LANE), F32),
        V((T + 2 * BLK, kvw), BF16), V((kvw, T + 2 * BLK), BF16),
        V((xw // LANE, T + 2 * EDGE, LANE), F32),
        V((nb, kvw, qw // HEAD * BLK), BF16), V((nb, gw, BLK), F32),
        V((T, 2 * state_w), BF16), V((nb, inner_w, BLK), BF16),
        V((nb, hd2, BLK), F32), V((nb, hd2, BLK), F32), V((nb, hd2, BLK), F32), V((nb, hd2, BLK), F32),
        V((inner_w, LANE), F32), V((2, BLK, BLK), F32),
        V((nb, 2, inner_w, STATE), F32), V((2, inner_w, STATE), F32), V((nb, hd2, LANE), F32),
        V((nb, 2, inner_w, STATE), BF16),
        V((T, qw + inner_w), BF16),
        V((T // 2, width), BF16), V((T // 2, width), BF16), V((T // 2, width), BF16),
        V((2, xw // LANE, EDGE, LANE), F32),
        V((2, inner_w, STATE), BF16), V((2, inner_w, STATE), BF16),
        dma((9,)), dma((nchunk,)), dma((nchunk,)), dma((nchunk,)),
        dma((6,)), dma((6,)), dma((2 * groups,)), dma((2 * groups,)), dma((steps,)), dma((steps,)),
        dma((steps,)),
    ]
    return pl.pallas_call(
        functools.partial(kernel, n_sp=n_sp),
        out_shape=jax.ShapeDtypeStruct((T // 2, width), BF16),
        in_specs=[any_spec] * 10 + [vm] * 18,
        out_specs=any_spec,
        scratch_shapes=scratch,
        compiler_params=pltpu.CompilerParams(
            collective_id=0, has_side_effects=True, vmem_limit_bytes=67043328
        ),
        name="mixer",
    )(
        inputs, w_query, w_key, w_value, w_inner, w_bmat, w_cmat, w_gate,
        w_out_attn, w_out_state, ws,
        mix_gain.reshape(1, -1), query_gain.reshape(1, -1), key_gain.reshape(1, -1),
        sink_logit.reshape(1, -1), conv_inner, conv_bmat, conv_cmat, step_bias, decay_rate,
        offs, start,
        group_gain.reshape(1, -1), jnp.asarray(ct), jnp.asarray(sn), jnp.asarray(co),
        jnp.asarray(so), jnp.asarray(tri).astype(BF16),
    )


def solution(mesh):
    return jax.shard_map(
        functools.partial(local, mesh.shape["sp"]),
        mesh=mesh,
        in_specs=(
            P(("fs", "sp"), "tp"),
            P(),
            P(None, "tp"),
            P(None, "tp"),
            P(None, "tp"),
            P(),
            P(),
            P("tp"),
            P(None, "tp"),
            P(None, "tp"),
            P(None, "tp"),
            P(None, "tp"),
            P(None, None, "tp"),
            P(None, "tp"),
            P(None, "tp"),
            P(None, "tp"),
            P(None, "tp"),
            P(None, "tp"),
            P("sp", None, "tp"),
            P("fs", "tp", None, None),
            P("tp"),
            P("tp", None),
            P("tp", None),
        ),
        out_specs=P(("fs", "sp", "tp"), None),
        check_vma=False,
    )
```

time: 76.4 us -> 57.6 us (0.75)
  Pallas kernels: 69.3 us -> 54.3 us
  local copies, waits for them, and re-layouts: 6.84 us -> 3.16 us
    pallas_call x1, Pallas kernels: 69.3 us -> 54.3 us  [local(): pl.pallas_call(functools.partial(kernel, n_sp=n_sp), out_shape=jax.ShapeD...]
    reshape x2 -> x0, local copies, waits for them, and re-layouts: 3.68 us -> none  [the longest x1 1.84 us: local(): ws = w_step.reshape(depth, -1)]
where the time goes in v1:
time: 57.6 us; the launch traced here: 57.5 us
  Pallas kernels  54.3 us (94%)
  local copies, waits for them, and re-layouts  3.16 us (5%)
    pallas_call x1, Pallas kernels, local(): pl.pallas_call(functools.partial(kernel, n_sp=n_sp), out_shape=jax.ShapeD...  54.3 us
    unnamed x1, local copies, waits for them, and re-layouts  3.16 us

profile of v1, /device:TPU:0, one launch (start us, length us, event | category | flops | bytes accessed | tf_op | source)
XLA Modules:
  0.0 57.5 jit_solution(16673266717310806878)
XLA Ops:
  0.0 54.3 %mixer.1 = bf16[512,2048]{1,0:T(8,128)(2,1)} custom-call(bf16[1024,1024]{1,0:T(8,128)(2,1)} %x_hbm.1, bf16[2048,512]{1,0:T(8,128)(2,1)} %wq.1, bf16[2048,128]{1,0:T(8,128)(2,1)} %wk.1, bf16[2048,128]{1,0:T(8,128)(2,1)} %wv.1, bf16[2048,512]{1,0:T(8,128)(2,1)} %wi.1, bf16[2048,256]{1,0:T(8,128)(2,1)} %wb.1, bf16[2048,256]{1,0:T(8,128)(2,1)} %wc.1, ...), custom_call_target="tpu_custom_call" | custom-call | tf_op jit(solution)/shard_map/mixer/pallas_call | solution.py:717
  54.3 3.2 %copy.30 = bf16[512,2048]{1,0:T(8,128)(2,1)} copy(bf16[512,2048]{1,0:T(8,128)(2,1)} %mixer.1) | data formatting | bytes 4194304

commit v2 on v1

v2 whole, which is shorter than its diff:
```python
import functools

import jax
import jax.numpy as jnp
import numpy as np
from jax import lax
from jax.experimental import pallas as pl
from jax.experimental.pallas import tpu as pltpu
from jax.sharding import PartitionSpec as P

HEAD = 64
STATE = 128
CONV = 5
BLK = 128
LANE = 128
ROWS = 256
EDGE = 8

epsilon = 1e-06
rotary_base = 10000.0
LOG2E = 1.4426950408889634
NEG = -1e30
F32 = jnp.float32
BF16 = jnp.bfloat16
MESH = pl.DeviceIdType.MESH


def mm(a, b):
    return jnp.dot(a, b, preferred_element_type=F32)


def mm_t(a, b):
    return lax.dot_general(a, b, (((1,), (1,)), ((), ())), preferred_element_type=F32)


def silu(v):
    return v / (1.0 + jnp.exp(-v))


def rounded(v):
    return v.astype(BF16).astype(F32)


def column(row):
    return jnp.broadcast_to(row, (LANE, LANE)).T


def pad_row(row):
    return jnp.concatenate([row, jnp.zeros((1, LANE - row.shape[1]), F32)], axis=1)


def pieces(v):
    hi = v.astype(BF16)
    rest = v - hi.astype(F32)
    mid = rest.astype(BF16)
    lo = (rest - mid.astype(F32)).astype(BF16)
    return hi, mid, lo


def interleave(main, hosted):
    main = list(main)
    hosted = list(hosted)
    done = 0
    for i, step in enumerate(main):
        want = ((i + 1) * len(hosted)) // len(main)
        step()
        while done < want:
            hosted[done]()
            done += 1


def kernel(
    x_hbm, wq, wk, wv, wi, wb, wc, wg, woa, wos, start_hbm,
    ws_h, mix_gain_h, qgain_h, kgain_h, sink_h, taps_i_h, taps_b_h, taps_c_h, bias_h, rate_h, offs_h,
    ggain_h, cos_t_h, sin_t_h, cos_o_h, sin_o_h, tri_h,
    outv,
    ws, mix_gain, qgain1, kgain1, sink, taps_i, taps_b, taps_c, bias2, rate2, offs,
    ggain, cos_t, sin_t, cos_o, sin_o, tri,
    w, wsp, wo, start, xown, xpeer, xs, rs, rot, kn, vt, xb, qt, gt, bc, xt, st, ct, dec, ld, ggt, bias_m,
    gs, agg, dtot, sb, z, psend, precv, xhalo, chain_s, chain_r,
    sem_v, sem_w, sem_x, sem_xs, sem_xr, sem_hs, sem_hr, sem_cs, sem_cr, sem_ps, sem_pr,
    *, n_sp,
):
    me = lax.axis_index("tp")
    idx = lax.axis_index("sp")
    peer = 1 - me
    T, half = x_hbm.shape
    nb = T // BLK
    nchunk = T // ROWS
    per = ROWS // BLK
    has_prev = idx > 0
    has_next = idx < n_sp - 1

    own_copies = []
    for i in range(nchunk):
        c = pltpu.make_async_copy(
            x_hbm.at[pl.ds(i * ROWS, ROWS)], xown.at[pl.ds(i * ROWS, ROWS)], sem_x.at[i]
        )
        c.start()
        own_copies.append(c)

    barrier = pltpu.get_barrier_semaphore()
    pl.semaphore_signal(barrier, inc=1, device_id={"tp": peer}, device_id_type=MESH)

    @pl.when(has_prev)
    def _():
        pl.semaphore_signal(barrier, inc=1, device_id={"sp": idx - 1}, device_id_type=MESH)

    @pl.when(has_next)
    def _():
        pl.semaphore_signal(barrier, inc=1, device_id={"sp": idx + 1}, device_id_type=MESH)

    small = []
    for j, (src, dst) in enumerate((
        (mix_gain_h, mix_gain), (qgain_h, qgain1), (kgain_h, kgain1), (cos_o_h, cos_o), (sin_o_h, sin_o),
        (cos_t_h, cos_t), (sin_t_h, sin_t), (bias_h, bias2), (rate_h, rate2), (ggain_h, ggain), (ws_h, ws),
        (sink_h, sink), (taps_i_h, taps_i), (taps_b_h, taps_b), (taps_c_h, taps_c), (offs_h, offs),
        (tri_h, tri),
    )):
        c = pltpu.make_async_copy(src, dst, sem_v.at[j])
        c.start()
        small.append(c)
    wcopies = []
    col = 0
    for j, src in enumerate((wi, wb, wc, wk, wv, wq, wg)):
        width = src.shape[1]
        wcopies.append(pltpu.make_async_copy(src, w.at[:, pl.ds(col, width)], sem_w.at[j]))
        col += width
    for c in wcopies[:3]:
        c.start()
    n_w = len(wcopies)
    na = woa.shape[0]
    oc = [
        pltpu.make_async_copy(woa, wo.at[pl.ds(0, na)], sem_w.at[n_w]),
        pltpu.make_async_copy(wos, wo.at[pl.ds(na, wos.shape[0])], sem_w.at[n_w + 1]),
        pltpu.make_async_copy(start_hbm, start, sem_w.at[n_w + 2]),
    ]

    inner_w = wi.shape[1]
    state_w = wb.shape[1]
    xw = inner_w + 2 * state_w
    kvw = wk.shape[1]
    qw = wq.shape[1]
    gw = wg.shape[1]
    kvcol = xw
    qcol = xw + 2 * kvw
    gcol = qcol + qw
    hd2 = ws.shape[0]
    heads = hd2 // 2
    groups = state_w // STATE
    per_group = heads // groups
    gwid = per_group * HEAD
    kv_heads = kvw // HEAD
    q_per = (qw // HEAD) // kv_heads
    two = LANE // HEAD
    sq = (BLK, BLK)
    ri = lax.broadcasted_iota(jnp.int32, sq, 0)
    ci = lax.broadcasted_iota(jnp.int32, sq, 1)

    wsp[hd2:, :] = jnp.zeros((LANE - hd2, wsp.shape[1]), BF16)
    qt[...] = jnp.zeros_like(qt)
    bias_m[0] = jnp.where(ri >= ci, 0.0, NEG)
    bias_m[1] = jnp.where(ri <= ci, 0.0, NEG)
    for c in small:
        c.wait()
    wsp[0:hd2, :] = ws[...]
    qg = column(pad_row(qgain1[...] * (HEAD ** (-0.5) * LOG2E)))
    kg = column(pad_row(kgain1[...]))
    hh = HEAD // 2
    co = cos_o[idx]
    so = sin_o[idx]
    for b in range(nb):
        cols = slice(b * BLK, (b + 1) * BLK)
        c0 = cos_t[:, cols]
        s0 = sin_t[:, cols]
        cosine = co * c0 - so * s0
        sine = so * c0 + co * s0
        for k, gain in enumerate((qg, kg)):
            ga, gb = gain[0:hh], gain[hh:HEAD]
            rot[k, b, 0:hh] = ga * cosine
            rot[k, b, hh : 2 * hh] = gb * sine
            rot[k, b, 2 * hh : 3 * hh] = gb * cosine
            rot[k, b, 3 * hh : 4 * hh] = ga * sine
    bias = column(pad_row(jnp.concatenate([bias2[0:1, :], bias2[1:2, :]], axis=1)))[0:hd2]
    rate = column(pad_row(jnp.concatenate([rate2[0:1, :], rate2[1:2, :]], axis=1)))[0:hd2]
    for s in range(0, inner_w, LANE):
        ggt[s : s + LANE, :] = column(ggain[:, s : s + LANE])

    @pl.when(has_prev & has_next)
    def _():
        pl.semaphore_wait(barrier, 3)

    @pl.when(jnp.logical_not(has_prev & has_next))
    def _():
        pl.semaphore_wait(barrier, 2 if n_sp > 1 else 1)

    gath = []
    for i in range(nchunk):
        own_copies[i].wait()
        c = pltpu.make_async_remote_copy(
            src_ref=xown.at[pl.ds(i * ROWS, ROWS)],
            dst_ref=xpeer.at[pl.ds(i * ROWS, ROWS)],
            send_sem=sem_xs.at[i],
            recv_sem=sem_xr.at[i],
            device_id={"tp": peer},
            device_id_type=MESH,
        )
        c.start()
        gath.append(c)
    for c in wcopies[3:]:
        c.start()

    gain_own = mix_gain[:, pl.ds(pl.multiple_of(me * half, LANE), half)]
    gain_peer = mix_gain[:, pl.ds(pl.multiple_of(peer * half, LANE), half)]

    def scale_rows(rows, n, src, gain, base, add):
        dst = pl.multiple_of(base * half, LANE)
        total = rs[rows, :] if add else jnp.zeros((n, LANE), F32)
        for s in range(0, half, LANE):
            a = src[rows, s : s + LANE].astype(F32)
            total = total + a * a
            xs[rows, pl.ds(pl.multiple_of(dst + s, LANE), LANE)] = (
                a * gain[:, s : s + LANE]
            ).astype(BF16)
        if add:
            total = jnp.broadcast_to(
                lax.rsqrt(jnp.sum(total, axis=1, keepdims=True) * (1.0 / (2 * half)) + epsilon), (n, LANE)
            )
        rs[rows, :] = total

    def scale_own(r, carry):
        scale_rows(pl.ds(pl.multiple_of(r * 32, 32), 32), 32, xown, gain_own, me, False)
        return carry

    def scale_peer(i):
        def piece(r):
            return lambda: scale_rows(slice(r, r + 32), 32, xpeer, gain_peer, peer, True)

        return [piece(r) for r in range(i * ROWS, (i + 1) * ROWS, 32)]

    lax.fori_loop(0, T // 32, scale_own, 0, unroll=2)
    gath[0].wait()
    for piece in scale_peer(0):
        piece()

    def norm_rotate(v, k, b):
        inv = lax.rsqrt(jnp.sum(v * v, axis=0, keepdims=True) * (1.0 / HEAD) + epsilon)
        a, c = v[0:hh], v[hh:HEAD]
        first = (a * rot[k, b, 0:hh] - c * rot[k, b, hh : 2 * hh]) * inv
        second = (c * rot[k, b, 2 * hh : 3 * hh] + a * rot[k, b, 3 * hh : 4 * hh]) * inv
        return jnp.concatenate([first, second], axis=0)

    def remote(src, dst, ss, rsem, target):
        return pltpu.make_async_remote_copy(
            src_ref=src, dst_ref=dst, send_sem=ss, recv_sem=rsem,
            device_id={"sp": target}, device_id_type=MESH,
        )

    def chunk_rows(i):
        return pl.ds(pl.multiple_of(i * ROWS, ROWS), ROWS)

    def x_units(i):
        rows = chunk_rows(i)

        def step_unit():
            p = mm_t(xs[rows, :], wsp[...]) * rs[rows, :]
            pt = p.T[0:hd2]
            for u in range(per):
                b = i * per + u
                v = pt[:, u * BLK : (u + 1) * BLK] + bias
                step = jnp.maximum(v, 0.0) + jnp.log1p(jnp.exp(-jnp.abs(v)))
                st[b] = step
                ld[b] = -rate * step + offs[:, b * BLK : (b + 1) * BLK]

        def unit(s):
            def run():
                p = mm(xs[rows, :], w[:, s : s + 256])
                for t in range(0, 256, LANE):
                    xb[(s + t) // LANE, pl.ds(i * ROWS + EDGE, ROWS), :] = rounded(
                        p[:, t : t + LANE] * rs[rows, :]
                    )
            return run

        return [step_unit] + [unit(s) for s in range(0, xw, 256)]

    def kv_unit(i):
        def run():
            rows = chunk_rows(i)
            p = mm(xs[rows, :], w[:, kvcol : kvcol + 2 * kvw])
            for u in range(per):
                b = i * per + u
                part = slice(u * BLK, (u + 1) * BLK)
                scale = rs[i * ROWS + u * BLK : i * ROWS + (u + 1) * BLK, :]
                kt = rounded(p[part, :LANE] * scale).T
                kt = jnp.concatenate(
                    [norm_rotate(kt[h * HEAD : (h + 1) * HEAD], 1, b) for h in range(kv_heads)], axis=0
                )
                dst = (b + 1) * BLK
                kn[dst : dst + BLK, :] = kt.T.astype(BF16)
                vt[:, dst : dst + BLK] = (p[part, LANE:] * scale).T.astype(BF16)
        return run

    def q_units(i):
        rows = chunk_rows(i)

        def unit(s):
            def run():
                p = mm(xs[rows, :], w[:, qcol + s : qcol + s + 256])
                scale = rs[rows, :]
                for u in range(per):
                    b = i * per + u
                    part = slice(u * BLK, (u + 1) * BLK)
                    for t in range(0, 256, LANE):
                        q = rounded(p[part, t : t + LANE] * scale[part]).T
                        for v in range(two):
                            h = (s + t) // HEAD + v
                            g = h // q_per
                            qt[b, g * HEAD : (g + 1) * HEAD, h * BLK : (h + 1) * BLK] = norm_rotate(
                                q[v * HEAD : (v + 1) * HEAD], 0, b
                            ).astype(BF16)
            return run

        return [unit(s) for s in range(0, qw, 256)]

    def gate_units(i):
        rows = chunk_rows(i)

        def unit(s):
            def run():
                p = mm(xs[rows, :], w[:, gcol + s : gcol + s + 256])
                scale = rs[rows, :]
                for u in range(per):
                    part = slice(u * BLK, (u + 1) * BLK)
                    for t in range(0, 256, LANE):
                        gt[i * per + u, s + t : s + t + LANE, :] = silu(
                            rounded(p[part, t : t + LANE] * scale[part]).T
                        )
            return run

        return [unit(s) for s in range(0, gw, 256)]

    def spread(values, row, n):
        return jnp.broadcast_to(values[row : row + 1, :], (n, LANE))

    def decay_block(b):
        sums = mm(jnp.concatenate(list(pieces(ld[b])), axis=0), tri[...])
        tot = (sums[0:hd2] + sums[hd2 : 2 * hd2] + sums[2 * hd2 : 3 * hd2]) * LOG2E
        c = jnp.concatenate([tot[0:heads, 0:BLK], tot[heads:, BLK:]], axis=0)
        ct[b] = c
        end = jnp.concatenate(
            [
                jnp.broadcast_to(c[0:heads, BLK - 1 : BLK], (heads, BLK)),
                jnp.broadcast_to(c[heads:, 0:1], (heads, BLK)),
            ],
            axis=0,
        )
        dec[b] = jnp.exp2(end)
        ld[b] = st[b] * jnp.exp2(end - c)

    def state_steps(b):
        rows = slice(b * BLK, (b + 1) * BLK)

        def tile_step(tile):
            s = tile * LANE

            def run():
                if s < inner_w:
                    tap = taps_i[:, s : s + LANE].astype(F32)
                elif s < inner_w + state_w:
                    tap = taps_b[:, s - inner_w : s - inner_w + LANE].astype(F32)
                else:
                    o = s - inner_w - state_w
                    tap = taps_c[:, o : o + LANE].astype(F32)
                acc = None
                for j in range(CONV):
                    win = xb[tile, pl.ds(b * BLK + (EDGE - CONV // 2 + j), BLK), :]
                    term = win * tap[j : j + 1]
                    acc = term if acc is None else acc + term
                a = silu(acc)
                if s >= inner_w:
                    bc[rows, s - inner_w : s - inner_w + LANE] = a.astype(BF16)
                    return
                at = rounded(a.T)
                xt[b, s : s + LANE, :] = at.astype(BF16)
                g = s // gwid
                load = ld[b]
                loaded = []
                for direction in range(2):
                    for u in range(two):
                        h = tile * two + u
                        loaded.append(
                            (at[u * HEAD : (u + 1) * HEAD] * spread(load, direction * heads + h, HEAD)).astype(BF16)
                        )
                gsum = mm(jnp.concatenate(loaded, axis=0), bc[rows, g * STATE : (g + 1) * STATE])
                for direction in range(2):
                    gs[b, direction, s : s + LANE, :] = gsum[direction * LANE : (direction + 1) * LANE]
            return run

        def first():
            decay_block(b)

        order = list(range(inner_w // LANE, xw // LANE)) + list(range(inner_w // LANE))
        return [first] + [tile_step(t) for t in order]

    x_up = remote(xb.at[:, pl.ds(T, EDGE)], xhalo.at[0], sem_hs.at[2], sem_hr.at[2], idx + 1)
    x_dn = remote(xb.at[:, pl.ds(EDGE, EDGE)], xhalo.at[1], sem_hs.at[3], sem_hr.at[3], idx - 1)
    k_up = remote(kn.at[pl.ds(T, BLK)], kn.at[pl.ds(0, BLK)], sem_hs.at[0], sem_hr.at[0], idx + 1)
    k_dn = remote(kn.at[pl.ds(BLK, BLK)], kn.at[pl.ds(T + BLK, BLK)], sem_hs.at[1], sem_hr.at[1], idx - 1)
    v_up = remote(vt.at[:, pl.ds(T, BLK)], vt.at[:, pl.ds(0, BLK)], sem_hs.at[4], sem_hr.at[4], idx + 1)
    v_dn = remote(vt.at[:, pl.ds(BLK, BLK)], vt.at[:, pl.ds(T + BLK, BLK)], sem_hs.at[5], sem_hr.at[5], idx - 1)

    for c in wcopies[:3]:
        c.wait()
    for c in oc:
        c.start()

    pending = [b for b in range(1, nb - 1)]
    for i in range(nchunk):
        hosted = []
        if i + 1 < nchunk:
            gath[i + 1].wait()
            hosted += scale_peer(i + 1)
        ready = [b for b in pending if (b + 1) * BLK + CONV // 2 <= i * ROWS][:per]
        for b in ready:
            pending.remove(b)
            hosted += state_steps(b)
        with jax.named_scope("x"):
            interleave(x_units(i), hosted)
        if i == 0:
            @pl.when(has_prev)
            def _():
                x_dn.start()

    @pl.when(has_next)
    def _():
        x_up.start()

    for c in wcopies[3:]:
        c.wait()

    with jax.named_scope("kv"):
        hosted = []
        for b in pending:
            hosted += state_steps(b)
        interleave([kv_unit(i) for i in range(nchunk)], hosted)

    @pl.when(has_next)
    def _():
        k_up.start()
        v_up.start()

    @pl.when(has_prev)
    def _():
        k_dn.start()
        v_dn.start()

    @pl.when(has_next)
    def _():
        x_up.wait_send()
        x_dn.wait_recv()
        xb[:, pl.ds(T + EDGE, EDGE), :] = xhalo[1]

    @pl.when(jnp.logical_not(has_next))
    def _():
        xb[:, pl.ds(T + EDGE, EDGE), :] = jnp.zeros((xb.shape[0], EDGE, LANE), F32)

    @pl.when(has_prev)
    def _():
        x_dn.wait_send()
        x_up.wait_recv()
        xb[:, pl.ds(0, EDGE), :] = xhalo[0]

    @pl.when(jnp.logical_not(has_prev))
    def _():
        xb[:, pl.ds(0, EDGE), :] = jnp.zeros((xb.shape[0], EDGE, LANE), F32)

    with jax.named_scope("edge"):
        interleave(q_units(0), state_steps(0) + (state_steps(nb - 1) if nb > 1 else []))

    for d in range(2):
        order = list(range(nb)) if d == 0 else list(range(nb - 1, -1, -1))
        for h in range(heads):
            rows = slice(h * HEAD, (h + 1) * HEAD)
            total = gs[order[0], d, rows, :]
            for b in order[1:]:
                total = total * spread(dec[b], d * heads + h, HEAD) + gs[b, d, rows, :]
            agg[d, rows, :] = total
    prod = dec[0]
    for b in range(1, nb):
        prod = prod * dec[b]
    dtot[...] = prod

    oc[2].wait()
    hops = [
        [
            remote(
                chain_s.at[d, pl.ds(g * gwid, gwid)], chain_r.at[d, pl.ds(g * gwid, gwid)],
                sem_cs.at[d * groups + g], sem_cr.at[d * groups + g],
                idx + 1 if d == 0 else idx - 1,
            )
            for g in range(groups)
        ]
        for d in range(2)
    ]
    sources = (has_prev, has_next)
    targets = (has_next, has_prev)
    order_of = (idx, n_sp - 1 - idx)

    def hop(direction, inner):
        for g in range(groups):
            if inner:
                hops[direction][g].wait_recv()
            for u in range(per_group):
                h = g * per_group + u
                rows = slice(h * HEAD, (h + 1) * HEAD)
                enter = chain_r[direction, rows, :].astype(F32) if inner else start[direction, rows, :]
                out = enter * spread(dtot[...], direction * heads + h, HEAD) + agg[direction, rows, :]
                chain_s[direction, rows, :] = out.astype(BF16)
            hops[direction][g].start()

    for d in range(2):
        @pl.when(targets[d] & jnp.logical_not(sources[d]))
        def _(d=d):
            hop(d, False)

    slots = nchunk

    def maybe_hop(slot):
        with jax.named_scope("hop"):
            for d in range(2):
                turn = (order_of[d] * slots * 3 + 3) // (2 * n_sp)

                @pl.when((jnp.minimum(turn, slots) == slot) & targets[d] & sources[d])
                def _(d=d):
                    hop(d, True)

    @pl.when(has_next)
    def _():
        k_up.wait_send()
        v_up.wait_send()
        k_dn.wait_recv()
        v_dn.wait_recv()

    @pl.when(jnp.logical_not(has_next))
    def _():
        kn[pl.ds(T + BLK, BLK), :] = jnp.zeros((BLK, kvw), BF16)
        vt[:, pl.ds(T + BLK, BLK)] = jnp.zeros((kvw, BLK), BF16)

    @pl.when(has_prev)
    def _():
        k_dn.wait_send()
        v_dn.wait_send()
        k_up.wait_recv()
        v_up.wait_recv()

    @pl.when(jnp.logical_not(has_prev))
    def _():
        kn[pl.ds(0, BLK), :] = jnp.zeros((BLK, kvw), BF16)
        vt[:, pl.ds(0, BLK)] = jnp.zeros((kvw, BLK), BF16)

    key_w = 3 * BLK
    ones = jnp.ones((16, key_w), BF16)
    sinks = sink[...] * LOG2E
    pairs = qw // HEAD // 2

    def attend_chunk(i, hosted):
        todo = [(i * per + u, p) for u in range(per) for p in range(pairs)]
        los = {}

        def scores(n):
            b, p = todo[n]
            return mm(kn[b * BLK : b * BLK + key_w, :], qt[b, :, 2 * p * BLK : 2 * (p + 1) * BLK])

        def weigh(n, s_all):
            b, p = todo[n]
            lo, hi = bias_m[0], bias_m[1]
            if b == 0:
                lo = lo + jnp.where(idx == 0, NEG, 0.0)
            if b == nb - 1:
                hi = hi + jnp.where(idx == n_sp - 1, NEG, 0.0)
            probs, adds = [], []
            for u in range(2):
                h = 2 * p + u
                s = s_all[:, u * BLK : (u + 1) * BLK]
                s = jnp.concatenate([s[0:BLK] + lo, s[BLK : 2 * BLK], s[2 * BLK :] + hi], axis=0)
                sk = jnp.broadcast_to(sinks[:, h : h + 1], (1, BLK))
                m = jnp.maximum(jnp.max(s, axis=0, keepdims=True), sk)
                probs.append(jnp.exp2(s - m).astype(BF16))
                adds.append(jnp.exp2(sk - m))
            return jnp.concatenate(probs, axis=1), adds

        def value(n, probs, adds):
            b, p = todo[n]
            g = 2 * p // q_per
            vals = jnp.concatenate([vt[g * HEAD : (g + 1) * HEAD, b * BLK : b * BLK + key_w], ones], axis=0)
            o = mm(vals, probs)
            outs = []
            for u in range(2):
                cols = slice(u * BLK, (u + 1) * BLK)
                inv = 1.0 / (o[HEAD : HEAD + 1, cols] + adds[u])
                outs.append(o[0:HEAD, cols] * inv)
            z[b * BLK : (b + 1) * BLK, p * LANE : (p + 1) * LANE] = (
                jnp.concatenate(outs, axis=0).T.astype(BF16)
            )

        state = {0: scores(0)}

        def step(n):
            def run():
                if n + 1 < len(todo):
                    state[n + 1] = scores(n + 1)
                state[n] = weigh(n, state[n])
            return run

        def close(n):
            return lambda: value(n, *state.pop(n))

        done = 0
        for n in range(len(todo)):
            step(n)()
            want = ((n + 1) * len(hosted)) // len(todo)
            while done < want:
                hosted[done]()
                done += 1
            close(n)()

    for i in range(nchunk):
        maybe_hop(i)
        with jax.named_scope("attend"):
            attend_chunk(i, (q_units(i + 1) if i + 1 < nchunk else []) + gate_units(i))
    maybe_hop(nchunk)

    with jax.named_scope("w_chain"):
        for d in range(2):
            @pl.when(targets[d])
            def _(d=d):
                for c in hops[d]:
                    c.wait_send()

            @pl.when(sources[d] & jnp.logical_not(targets[d]))
            def _(d=d):
                for c in hops[d]:
                    c.wait_recv()

    for d in range(2):
        order = list(range(nb)) if d == 0 else list(range(nb - 1, -1, -1))
        for h in range(heads):
            rows = slice(h * HEAD, (h + 1) * HEAD)
            total = jnp.where(sources[d], chain_r[d, rows, :].astype(F32), start[d, rows, :])
            for b in order:
                sb[b, d, rows, :] = total.astype(BF16)
                if b != order[-1]:
                    total = total * spread(dec[b], d * heads + h, HEAD) + gs[b, d, rows, :]

    attn_w = qw
    zero_pad = jnp.zeros((LANE - hd2, LANE), F32)

    def mix_steps(b):
        rows = pl.ds(pl.multiple_of(b * BLK, BLK), BLK)
        env = {}

        def begin():
            c = ct[b]
            step = st[b]
            e = c - jnp.log2(jnp.maximum(step, 1e-37))
            env["c"] = c
            env["en"] = jnp.concatenate([e, zero_pad], axis=0).T
            env["both"] = jnp.log2(jnp.maximum(step[0:heads] + step[heads:], 1e-37))
            env["grow"] = jnp.exp2(c)

        def open_group(g):
            def run():
                bm = bc[rows, g * STATE : (g + 1) * STATE]
                cm = bc[rows, state_w + g * STATE : state_w + (g + 1) * STATE]
                env["scores"] = mm_t(bm, cm)
                states = jnp.concatenate(
                    [sb[b, d, g * gwid : (g + 1) * gwid, :] for d in range(2)], axis=0
                )
                env["carried"] = mm_t(states, cm)
                env["gated"] = []
            return run

        def head(g, u):
            def run():
                h = g * per_group + u
                c, en, carried, grow = env["c"], env["en"], env["carried"], env["grow"]
                arg = jnp.where(
                    ri < ci,
                    spread(c, h, BLK) - jnp.broadcast_to(en[:, h : h + 1], sq),
                    spread(c, heads + h, BLK) - jnp.broadcast_to(en[:, heads + h : heads + h + 1], sq),
                )
                arg = jnp.where(ri == ci, spread(env["both"], h, BLK), arg)
                weights = (env["scores"] * jnp.exp2(arg)).astype(BF16)
                y = mm(xt[b, h * HEAD : (h + 1) * HEAD, :], weights)
                y = y + carried[u * HEAD : (u + 1) * HEAD] * spread(grow, h, HEAD)
                y = y + carried[gwid + u * HEAD : gwid + (u + 1) * HEAD] * spread(grow, heads + h, HEAD)
                env["gated"].append(y * gt[b, h * HEAD : (h + 1) * HEAD, :])
            return run

        def close_group(g):
            def run():
                gated = env["gated"]
                total = sum(jnp.sum(v * v, axis=0, keepdims=True) for v in gated)
                inv = lax.rsqrt(total * (1.0 / gwid) + epsilon)
                for t in range(per_group // 2):
                    s = g * gwid + t * LANE
                    v = jnp.concatenate([gated[2 * t], gated[2 * t + 1]], axis=0)
                    z[rows, attn_w + s : attn_w + s + LANE] = (v * inv * ggt[s : s + LANE, :]).T.astype(BF16)
            return run

        steps = [begin]
        for g in range(groups):
            steps.append(open_group(g))
            steps += [head(g, u) for u in range(per_group)]
            steps.append(close_group(g))
        return steps

    for c in oc[:2]:
        c.wait()
    half_rows = T // 2
    steps = half_rows // ROWS
    width = wo.shape[1]
    copies = [
        pltpu.make_async_remote_copy(
            src_ref=psend.at[pl.ds(i * ROWS, ROWS)],
            dst_ref=precv.at[pl.ds(i * ROWS, ROWS)],
            send_sem=sem_ps.at[i],
            recv_sem=sem_pr.at[i],
            device_id={"tp": peer},
            device_id_type=MESH,
        )
        for i in range(steps)
    ]

    def chunk_base(k):
        owner = peer if k < steps else me
        return owner * half_rows + (k % steps) * ROWS

    def out_units(k):
        zr = pl.ds(pl.multiple_of(chunk_base(k), ROWS), ROWS)
        i = k % steps
        dst = slice(i * ROWS, (i + 1) * ROWS)

        def unit(s):
            def run():
                part = mm(z[zr, :], wo[:, s : s + 256])
                if k < steps:
                    psend[dst, s : s + 256] = part.astype(BF16)
                else:
                    outv[dst, s : s + 256] = (
                        rounded(part) + precv[dst, s : s + 256].astype(F32)
                    ).astype(BF16)
            return run

        return [unit(s) for s in range(0, width, 256)]

    total_chunks = 2 * steps
    for k in range(total_chunks + 1):
        if k > steps:
            with jax.named_scope("w_p"):
                copies[k - 1 - steps].wait()
        with jax.named_scope("mix"):
            hosted = out_units(k - 1) if k > 0 else []
            main = []
            if k < total_chunks:
                for u in range(per):
                    main += mix_steps(chunk_base(k) // BLK + u)
            if main:
                interleave(main, hosted)
            else:
                for piece in hosted:
                    piece()
        if 0 < k <= steps:
            copies[k - 1].start()


def tables(tokens, count):
    half = HEAD // 2
    frequency = rotary_base ** (-np.arange(half, dtype=np.float64) / half)
    inner = frequency[:, None] * np.arange(tokens, dtype=np.float64)[None, :]
    outer = np.arange(count, dtype=np.float64)[:, None] * tokens * frequency[None, :]
    outer = np.broadcast_to(outer[:, :, None], (count, half, LANE))
    return [f(a).astype(np.float32) for a in (inner, outer) for f in (np.cos, np.sin)]


def local(
    n_sp,
    inputs, mix_gain, w_query, w_key, w_value, query_gain, key_gain, sink_logit,
    w_inner, w_bmat, w_cmat, w_gate, w_step, conv_inner, conv_bmat, conv_cmat,
    step_bias, decay_rate, decay_offset, start_state, group_gain, w_out_attn, w_out_state,
):
    T, half = inputs.shape
    depth = w_query.shape[0]
    heads = w_step.shape[2]
    inner_w = w_inner.shape[1]
    state_w = w_bmat.shape[1]
    xw = inner_w + 2 * state_w
    kvw = w_key.shape[1]
    qw = w_query.shape[1]
    gw = w_gate.shape[1]
    width = w_out_attn.shape[1]
    nb = T // BLK
    nchunk = T // ROWS
    groups = state_w // STATE

    ws = jnp.transpose(w_step, (1, 2, 0)).reshape(2 * heads, depth)
    offs = jnp.transpose(decay_offset, (1, 2, 0)).reshape(2 * heads, T)
    start = start_state.reshape(2, inner_w, STATE)
    ct, sn, co, so = tables(T, n_sp)
    tri = np.triu(np.ones((BLK, BLK), np.float32))
    tri = np.concatenate([tri, tri.T], axis=1)
    any_spec = pl.BlockSpec(memory_space=pl.ANY)
    vm = pl.BlockSpec(memory_space=pltpu.VMEM)
    wcols = 2 * kvw + xw + qw + gw
    V = pltpu.VMEM
    dma = pltpu.SemaphoreType.DMA
    steps = T // 2 // ROWS
    hd2 = 2 * heads
    small = [
        ws, mix_gain.reshape(1, -1), query_gain.reshape(1, -1), key_gain.reshape(1, -1),
        sink_logit.reshape(1, -1), conv_inner, conv_bmat, conv_cmat, step_bias, decay_rate,
        offs, group_gain.reshape(1, -1), jnp.asarray(ct), jnp.asarray(sn), jnp.asarray(co),
        jnp.asarray(so), jnp.asarray(tri, dtype=BF16),
    ]
    scratch = [V(a.shape, a.dtype) for a in small] + [
        V((depth, wcols), BF16), V((LANE, depth), BF16),
        V((w_out_attn.shape[0] + w_out_state.shape[0], width), BF16),
        V((2, inner_w, STATE), F32),
        V((T, half), BF16), V((T, half), BF16), V((T, 2 * half), BF16), V((T, LANE), F32),
        V((2, nb, 2 * HEAD, LANE), F32),
        V((T + 2 * BLK, kvw), BF16), V((kvw, T + 2 * BLK), BF16),
        V((xw // LANE, T + 2 * EDGE, LANE), F32),
        V((nb, kvw, qw // HEAD * BLK), BF16), V((nb, gw, BLK), F32),
        V((T, 2 * state_w), BF16), V((nb, inner_w, BLK), BF16),
        V((nb, hd2, BLK), F32), V((nb, hd2, BLK), F32), V((nb, hd2, BLK), F32), V((nb, hd2, BLK), F32),
        V((inner_w, LANE), F32), V((2, BLK, BLK), F32),
        V((nb, 2, inner_w, STATE), F32), V((2, inner_w, STATE), F32), V((hd2, LANE), F32),
        V((nb, 2, inner_w, STATE), BF16),
        V((T, qw + inner_w), BF16),
        V((T // 2, width), BF16), V((T // 2, width), BF16),
        V((2, xw // LANE, EDGE, LANE), F32),
        V((2, inner_w, STATE), BF16), V((2, inner_w, STATE), BF16),
        dma((len(small),)), dma((10,)), dma((nchunk,)), dma((nchunk,)), dma((nchunk,)),
        dma((6,)), dma((6,)), dma((2 * groups,)), dma((2 * groups,)), dma((steps,)), dma((steps,)),
    ]
    return pl.pallas_call(
        functools.partial(kernel, n_sp=n_sp),
        out_shape=pltpu.VMEM((T // 2, width), BF16),
        in_specs=[any_spec] * (11 + len(small)),
        out_specs=vm,
        scratch_shapes=scratch,
        compiler_params=pltpu.CompilerParams(
            collective_id=0, has_side_effects=True, vmem_limit_bytes=58720256
        ),
        name="mixer",
    )(
        inputs, w_query, w_key, w_value, w_inner, w_bmat, w_cmat, w_gate,
        w_out_attn, w_out_state, start, *small,
    )


def solution(mesh):
    return jax.shard_map(
        functools.partial(local, mesh.shape["sp"]),
        mesh=mesh,
        in_specs=(
            P(("fs", "sp"), "tp"),
            P(),
            P(None, "tp"),
            P(None, "tp"),
            P(None, "tp"),
            P(),
            P(),
            P("tp"),
            P(None, "tp"),
            P(None, "tp"),
            P(None, "tp"),
            P(None, "tp"),
            P(None, None, "tp"),
            P(None, "tp"),
            P(None, "tp"),
            P(None, "tp"),
            P(None, "tp"),
            P(None, "tp"),
            P("sp", None, "tp"),
            P("fs", "tp", None, None),
            P("tp"),
            P("tp", None),
            P("tp", None),
        ),
        out_specs=P(("fs", "sp", "tp"), None),
        check_vma=False,
    )
```

time: 57.6 us -> 46.4 us (0.81)
  Pallas kernels: 54.3 us -> 44.9 us
  local copies, waits for them, and re-layouts: 3.16 us -> 1.32 us
    pallas_call x1, Pallas kernels: 54.3 us -> 44.9 us  [local(): pl.pallas_call(functools.partial(kernel, n_sp=n_sp), out_shape=pltpu.VMEM...]
    unnamed x1, local copies, waits for them, and re-layouts: 3.16 us -> 1.32 us
where the time goes in v2:
time: 46.4 us; the launch traced here: 46.2 us
  Pallas kernels  44.9 us (97%)
  local copies, waits for them, and re-layouts  1.32 us (3%)
    pallas_call x1, Pallas kernels, local(): pl.pallas_call(functools.partial(kernel, n_sp=n_sp), out_shape=pltpu.VMEM...  44.9 us
    unnamed x1, local copies, waits for them, and re-layouts  1.32 us

profile of v2, /device:TPU:0, one launch (start us, length us, event | category | flops | bytes accessed | tf_op | source)
XLA Modules:
  0.0 46.2 jit_solution(14540543866378203737)
XLA Ops:
  0.0 44.9 %mixer.1 = bf16[512,2048]{1,0:T(8,128)(2,1)S(1)} custom-call(bf16[1024,1024]{1,0:T(8,128)(2,1)} %x_hbm.1, bf16[2048,512]{1,0:T(8,128)(2,1)} %wq.1, bf16[2048,128]{1,0:T(8,128)(2,1)} %wk.1, bf16[2048,128]{1,0:T(8,128)(2,1)} %wv.1, bf16[2048,512]{1,0:T(8,128)(2,1)} %wi.1, bf16[2048,256]{1,0:T(8,128)(2,1)} %wb.1, bf16[2048,256]{1,0:T(8,128)(2,1)} %wc.1, ...), custom_call_target="tpu_custom_call" | custom-call | tf_op jit(solution)/shard_map/mixer/pallas_call | solution.py:846
  44.9 1.3 %copy.30 = bf16[512,2048]{1,0:T(8,128)(2,1)} copy(bf16[512,2048]{1,0:T(8,128)(2,1)S(1)} %mixer.1) | data formatting | bytes 4194304

commit v3 on v2

--- a/solution.py
+++ b/solution.py
@@ -33,8 +33,8 @@
     return lax.dot_general(a, b, (((1,), (1,)), ((), ())), preferred_element_type=F32)
 
 
-def silu(v):
-    return v / (1.0 + jnp.exp(-v))
+def silu_of_twice(v):
+    return v + v * jnp.tanh(v)
 
 
 def rounded(v):
@@ -57,16 +57,25 @@
     return hi, mid, lo
 
 
-def interleave(main, hosted):
-    main = list(main)
-    hosted = list(hosted)
-    done = 0
-    for i, step in enumerate(main):
-        want = ((i + 1) * len(hosted)) // len(main)
-        step()
-        while done < want:
-            hosted[done]()
-            done += 1
+def pipeline(items):
+    active = []
+    for item in items:
+        stages = item()
+        if stages is None:
+            continue
+        active = [g for g in active + [stages] if next(g, True) is None]
+    while active:
+        active = [g for g in active if next(g, True) is None]
+
+
+def blend(main, extra):
+    out, done = [], 0
+    for i, item in enumerate(main):
+        out.append(item)
+        want = ((i + 1) * len(extra)) // len(main)
+        out += extra[done:want]
+        done = want
+    return out + extra[done:]
 
 
 def kernel(
@@ -76,11 +85,12 @@
     outv,
     ws, mix_gain, qgain1, kgain1, sink, taps_i, taps_b, taps_c, bias2, rate2, offs,
     ggain, cos_t, sin_t, cos_o, sin_o, tri,
-    w, wsp, wo, start, xown, xpeer, xs, rs, rot, kn, vt, xb, qt, gt, bc, xt, st, ct, dec, ld, ggt, bias_m,
-    gs, agg, dtot, sb, z, psend, precv, xhalo, chain_s, chain_r,
+    w, wsp, wo, start, xown, xpeer, xa, xp, rs, rot, kn, vt, xb, qt, gt, bc, xt, st, ct, dec, ld, ggt, bias_m,
+    gs, agg, dtot, sb, ys, z, zs0, zs1, zs2, zs3, psend, precv, xhalo, chain_s, chain_r,
     sem_v, sem_w, sem_x, sem_xs, sem_xr, sem_hs, sem_hr, sem_cs, sem_cr, sem_ps, sem_pr,
     *, n_sp,
 ):
+    zs = (zs0, zs1, zs2, zs3)
     me = lax.axis_index("tp")
     idx = lax.axis_index("sp")
     peer = 1 - me
@@ -91,13 +101,15 @@
     has_prev = idx > 0
     has_next = idx < n_sp - 1
 
-    own_copies = []
-    for i in range(nchunk):
+    first = [0] + ([nchunk - 1] if nchunk > 1 else [])
+    trail = first + [i for i in range(nchunk) if i not in first]
+    own_copies = {}
+    for i in trail:
         c = pltpu.make_async_copy(
             x_hbm.at[pl.ds(i * ROWS, ROWS)], xown.at[pl.ds(i * ROWS, ROWS)], sem_x.at[i]
         )
         c.start()
-        own_copies.append(c)
+        own_copies[i] = c
 
     barrier = pltpu.get_barrier_semaphore()
     pl.semaphore_signal(barrier, inc=1, device_id={"tp": peer}, device_id_type=MESH)
@@ -122,11 +134,18 @@
         small.append(c)
     wcopies = []
     col = 0
+    own_rows = pl.ds(pl.multiple_of(me * half, LANE), half)
+    peer_rows = pl.ds(pl.multiple_of(peer * half, LANE), half)
     for j, src in enumerate((wi, wb, wc, wk, wv, wq, wg)):
         width = src.shape[1]
-        wcopies.append(pltpu.make_async_copy(src, w.at[:, pl.ds(col, width)], sem_w.at[j]))
+        for k, part in enumerate((own_rows, peer_rows)):
+            wcopies.append(
+                pltpu.make_async_copy(
+                    src.at[part], w.at[pl.ds(k * half, half), pl.ds(col, width)], sem_w.at[2 * j + k]
+                )
+            )
         col += width
-    for c in wcopies[:3]:
+    for c in wcopies[:6]:
         c.start()
     n_w = len(wcopies)
     na = woa.shape[0]
@@ -163,7 +182,8 @@
     bias_m[1] = jnp.where(ri <= ci, 0.0, NEG)
     for c in small:
         c.wait()
-    wsp[0:hd2, :] = ws[...]
+    wsp[0:hd2, 0:half] = ws[:, own_rows]
+    wsp[0:hd2, half:] = ws[:, peer_rows]
     qg = column(pad_row(qgain1[...] * (HEAD ** (-0.5) * LOG2E)))
     kg = column(pad_row(kgain1[...]))
     hh = HEAD // 2
@@ -194,8 +214,8 @@
     def _():
         pl.semaphore_wait(barrier, 2 if n_sp > 1 else 1)
 
-    gath = []
-    for i in range(nchunk):
+    gath = {}
+    for i in trail:
         own_copies[i].wait()
         c = pltpu.make_async_remote_copy(
             src_ref=xown.at[pl.ds(i * ROWS, ROWS)],
@@ -206,22 +226,19 @@
             device_id_type=MESH,
         )
         c.start()
-        gath.append(c)
-    for c in wcopies[3:]:
+        gath[i] = c
+    for c in wcopies[6:]:
         c.start()
 
     gain_own = mix_gain[:, pl.ds(pl.multiple_of(me * half, LANE), half)]
     gain_peer = mix_gain[:, pl.ds(pl.multiple_of(peer * half, LANE), half)]
 
-    def scale_rows(rows, n, src, gain, base, add):
-        dst = pl.multiple_of(base * half, LANE)
+    def scale_rows(rows, n, src, gain, dst, add):
         total = rs[rows, :] if add else jnp.zeros((n, LANE), F32)
         for s in range(0, half, LANE):
             a = src[rows, s : s + LANE].astype(F32)
             total = total + a * a
-            xs[rows, pl.ds(pl.multiple_of(dst + s, LANE), LANE)] = (
-                a * gain[:, s : s + LANE]
-            ).astype(BF16)
+            dst[rows, s : s + LANE] = (a * gain[:, s : s + LANE]).astype(BF16)
         if add:
             total = jnp.broadcast_to(
                 lax.rsqrt(jnp.sum(total, axis=1, keepdims=True) * (1.0 / (2 * half)) + epsilon), (n, LANE)
@@ -229,12 +246,14 @@
         rs[rows, :] = total
 
     def scale_own(r, carry):
-        scale_rows(pl.ds(pl.multiple_of(r * 32, 32), 32), 32, xown, gain_own, me, False)
+        scale_rows(pl.ds(pl.multiple_of(r * 32, 32), 32), 32, xown, gain_own, xa, False)
         return carry
 
     def scale_peer(i):
         def piece(r):
-            return lambda: scale_rows(slice(r, r + 32), 32, xpeer, gain_peer, peer, True)
+            def run():
+                scale_rows(slice(r, r + 32), 32, xpeer, gain_peer, xp, True)
+            return run
 
         return [piece(r) for r in range(i * ROWS, (i + 1) * ROWS, 32)]
 
@@ -257,14 +276,18 @@
         )
 
     def chunk_rows(i):
-        return pl.ds(pl.multiple_of(i * ROWS, ROWS), ROWS)
+        return slice(i * ROWS, (i + 1) * ROWS)
+
+    def project(rows, lo, hi):
+        return mm(xa[rows, :], w[0:half, lo:hi]) + mm(xp[rows, :], w[half:, lo:hi])
 
     def x_units(i):
         rows = chunk_rows(i)
 
         def step_unit():
-            p = mm_t(xs[rows, :], wsp[...]) * rs[rows, :]
-            pt = p.T[0:hd2]
+            p = mm_t(xa[rows, :], wsp[:, 0:half]) + mm_t(xp[rows, :], wsp[:, half:])
+            yield
+            pt = (p * rs[rows, :]).T[0:hd2]
             for u in range(per):
                 b = i * per + u
                 v = pt[:, u * BLK : (u + 1) * BLK] + bias
@@ -274,7 +297,8 @@
 
         def unit(s):
             def run():
-                p = mm(xs[rows, :], w[:, s : s + 256])
+                p = project(rows, s, s + 256)
+                yield
                 for t in range(0, 256, LANE):
                     xb[(s + t) // LANE, pl.ds(i * ROWS + EDGE, ROWS), :] = rounded(
                         p[:, t : t + LANE] * rs[rows, :]
@@ -286,7 +310,8 @@
     def kv_unit(i):
         def run():
             rows = chunk_rows(i)
-            p = mm(xs[rows, :], w[:, kvcol : kvcol + 2 * kvw])
+            p = project(rows, kvcol, kvcol + 2 * kvw)
+            yield
             for u in range(per):
                 b = i * per + u
                 part = slice(u * BLK, (u + 1) * BLK)
@@ -305,7 +330,8 @@
 
         def unit(s):
             def run():
-                p = mm(xs[rows, :], w[:, qcol + s : qcol + s + 256])
+                p = project(rows, qcol + s, qcol + s + 256)
+                yield
                 scale = rs[rows, :]
                 for u in range(per):
                     b = i * per + u
@@ -327,13 +353,14 @@
 
         def unit(s):
             def run():
-                p = mm(xs[rows, :], w[:, gcol + s : gcol + s + 256])
+                p = project(rows, gcol + s, gcol + s + 256)
+                yield
                 scale = rs[rows, :]
                 for u in range(per):
                     part = slice(u * BLK, (u + 1) * BLK)
                     for t in range(0, 256, LANE):
-                        gt[i * per + u, s + t : s + t + LANE, :] = silu(
-                            rounded(p[part, t : t + LANE] * scale[part]).T
+                        gt[i * per + u, s + t : s + t + LANE, :] = silu_of_twice(
+                            0.5 * rounded(p[part, t : t + LANE] * scale[part]).T
                         )
             return run
 
@@ -344,6 +371,7 @@
 
     def decay_block(b):
         sums = mm(jnp.concatenate(list(pieces(ld[b])), axis=0), tri[...])
+        yield
         tot = (sums[0:hd2] + sums[hd2 : 2 * hd2] + sums[2 * hd2 : 3 * hd2]) * LOG2E
         c = jnp.concatenate([tot[0:heads, 0:BLK], tot[heads:, BLK:]], axis=0)
         ct[b] = c
@@ -365,18 +393,18 @@
 
             def run():
                 if s < inner_w:
-                    tap = taps_i[:, s : s + LANE].astype(F32)
+                    tap = 0.5 * taps_i[:, s : s + LANE].astype(F32)
                 elif s < inner_w + state_w:
-                    tap = taps_b[:, s - inner_w : s - inner_w + LANE].astype(F32)
+                    tap = 0.5 * taps_b[:, s - inner_w : s - inner_w + LANE].astype(F32)
                 else:
                     o = s - inner_w - state_w
-                    tap = taps_c[:, o : o + LANE].astype(F32)
+                    tap = 0.5 * taps_c[:, o : o + LANE].astype(F32)
                 acc = None
                 for j in range(CONV):
                     win = xb[tile, pl.ds(b * BLK + (EDGE - CONV // 2 + j), BLK), :]
                     term = win * tap[j : j + 1]
                     acc = term if acc is None else acc + term
-                a = silu(acc)
+                a = silu_of_twice(acc)
                 if s >= inner_w:
                     bc[rows, s - inner_w : s - inner_w + LANE] = a.astype(BF16)
                     return
@@ -391,13 +419,15 @@
                         loaded.append(
                             (at[u * HEAD : (u + 1) * HEAD] * spread(load, direction * heads + h, HEAD)).astype(BF16)
                         )
+                yield
                 gsum = mm(jnp.concatenate(loaded, axis=0), bc[rows, g * STATE : (g + 1) * STATE])
+                yield
                 for direction in range(2):
                     gs[b, direction, s : s + LANE, :] = gsum[direction * LANE : (direction + 1) * LANE]
             return run
 
         def first():
-            decay_block(b)
+            return decay_block(b)
 
         order = list(range(inner_w // LANE, xw // LANE)) + list(range(inner_w // LANE))
         return [first] + [tile_step(t) for t in order]
@@ -409,73 +439,97 @@
     v_up = remote(vt.at[:, pl.ds(T, BLK)], vt.at[:, pl.ds(0, BLK)], sem_hs.at[4], sem_hr.at[4], idx + 1)
     v_dn = remote(vt.at[:, pl.ds(BLK, BLK)], vt.at[:, pl.ds(T + BLK, BLK)], sem_hs.at[5], sem_hr.at[5], idx - 1)
 
-    for c in wcopies[:3]:
+    for c in wcopies[:6]:
         c.wait()
     for c in oc:
         c.start()
 
+    def action(f):
+        def run():
+            f()
+        return run
+
+    visit = list(range(1, nchunk - 1)) + [0] + ([nchunk - 1] if nchunk > 1 else [])
     pending = [b for b in range(1, nb - 1)]
-    for i in range(nchunk):
+
+    def send_rims():
+        @pl.when(has_prev)
+        def _():
+            x_dn.start()
+
+        @pl.when(has_next)
+        def _():
+            x_up.start()
+
+    def wait_rims():
+        @pl.when(has_next)
+        def _():
+            x_up.wait_send()
+            x_dn.wait_recv()
+            xb[:, pl.ds(T + EDGE, EDGE), :] = xhalo[1]
+
+        @pl.when(jnp.logical_not(has_next))
+        def _():
+            xb[:, pl.ds(T + EDGE, EDGE), :] = jnp.zeros((xb.shape[0], EDGE, LANE), F32)
+
+        @pl.when(has_prev)
+        def _():
+            x_dn.wait_send()
+            x_up.wait_recv()
+            xb[:, pl.ds(0, EDGE), :] = xhalo[0]
+
+        @pl.when(jnp.logical_not(has_prev))
+        def _():
+            xb[:, pl.ds(0, EDGE), :] = jnp.zeros((xb.shape[0], EDGE, LANE), F32)
+
+    seq = []
+    done = []
+    for n, i in enumerate(trail):
         hosted = []
-        if i + 1 < nchunk:
-            gath[i + 1].wait()
-            hosted += scale_peer(i + 1)
-        ready = [b for b in pending if (b + 1) * BLK + CONV // 2 <= i * ROWS][:per]
+        if n + 1 < nchunk:
+            seq.append(action(gath[trail[n + 1]].wait))
+            hosted += scale_peer(trail[n + 1])
+        ready = [
+            b for b in pending
+            if (b * BLK - CONV // 2) // ROWS in done and ((b + 1) * BLK + CONV // 2 - 1) // ROWS in done
+        ][:per]
         for b in ready:
             pending.remove(b)
             hosted += state_steps(b)
-        with jax.named_scope("x"):
-            interleave(x_units(i), hosted)
-        if i == 0:
-            @pl.when(has_prev)
-            def _():
-                x_dn.start()
-
-    @pl.when(has_next)
-    def _():
-        x_up.start()
-
-    for c in wcopies[3:]:
+        units = blend(x_units(i), hosted)
+        if n == len(first):
+            units.insert(2, action(send_rims))
+        seq += units
+        done.append(i)
+    with jax.named_scope("x"):
+        pipeline(seq)
+    if nchunk <= len(first):
+        send_rims()
+
+    for c in wcopies[6:]:
         c.wait()
 
+    def send_kv():
+        @pl.when(has_next)
+        def _():
+            k_up.start()
+            v_up.start()
+
+        @pl.when(has_prev)
+        def _():
+            k_dn.start()
+            v_dn.start()
+
+    inner_steps = []
+    for b in pending:
+        inner_steps += state_steps(b)
+    seq = blend(inner_steps, [kv_unit(i) for i in range(nchunk)])
+    rims = blend(
+        state_steps(0) + (state_steps(nb - 1) if nb > 1 else []), q_units(visit[0])
+    )
+    rims.insert(2, action(send_kv))
     with jax.named_scope("kv"):
-        hosted = []
-        for b in pending:
-            hosted += state_steps(b)
-        interleave([kv_unit(i) for i in range(nchunk)], hosted)
-
-    @pl.when(has_next)
-    def _():
-        k_up.start()
-        v_up.start()
-
-    @pl.when(has_prev)
-    def _():
-        k_dn.start()
-        v_dn.start()
-
-    @pl.when(has_next)
-    def _():
-        x_up.wait_send()
-        x_dn.wait_recv()
-        xb[:, pl.ds(T + EDGE, EDGE), :] = xhalo[1]
-
-    @pl.when(jnp.logical_not(has_next))
-    def _():
-        xb[:, pl.ds(T + EDGE, EDGE), :] = jnp.zeros((xb.shape[0], EDGE, LANE), F32)
-
-    @pl.when(has_prev)
-    def _():
-        x_dn.wait_send()
-        x_up.wait_recv()
-        xb[:, pl.ds(0, EDGE), :] = xhalo[0]
-
-    @pl.when(jnp.logical_not(has_prev))
-    def _():
-        xb[:, pl.ds(0, EDGE), :] = jnp.zeros((xb.shape[0], EDGE, LANE), F32)
-
-    with jax.named_scope("edge"):
-        interleave(q_units(0), state_steps(0) + (state_steps(nb - 1) if nb > 1 else []))
+        pipeline(seq + [action(wait_rims)] + rims)
 
     for d in range(2):
         order = list(range(nb)) if d == 0 else list(range(nb - 1, -1, -1))
@@ -528,51 +582,46 @@
     def maybe_hop(slot):
         with jax.named_scope("hop"):
             for d in range(2):
-                turn = (order_of[d] * slots * 3 + 3) // (2 * n_sp)
+                turn = jnp.maximum((order_of[d] * slots * 2) // n_sp, 1)
 
                 @pl.when((jnp.minimum(turn, slots) == slot) & targets[d] & sources[d])
                 def _(d=d):
                     hop(d, True)
 
-    @pl.when(has_next)
-    def _():
-        k_up.wait_send()
-        v_up.wait_send()
-        k_dn.wait_recv()
-        v_dn.wait_recv()
-
-    @pl.when(jnp.logical_not(has_next))
-    def _():
-        kn[pl.ds(T + BLK, BLK), :] = jnp.zeros((BLK, kvw), BF16)
-        vt[:, pl.ds(T + BLK, BLK)] = jnp.zeros((kvw, BLK), BF16)
-
-    @pl.when(has_prev)
-    def _():
-        k_dn.wait_send()
-        v_dn.wait_send()
-        k_up.wait_recv()
-        v_up.wait_recv()
-
-    @pl.when(jnp.logical_not(has_prev))
-    def _():
-        kn[pl.ds(0, BLK), :] = jnp.zeros((BLK, kvw), BF16)
-        vt[:, pl.ds(0, BLK)] = jnp.zeros((kvw, BLK), BF16)
+    def kv_halo():
+        @pl.when(has_next)
+        def _():
+            k_up.wait_send()
+            v_up.wait_send()
+            k_dn.wait_recv()
+            v_dn.wait_recv()
+
+        @pl.when(jnp.logical_not(has_next))
+        def _():
+            kn[pl.ds(T + BLK, BLK), :] = jnp.zeros((BLK, kvw), BF16)
+            vt[:, pl.ds(T + BLK, BLK)] = jnp.zeros((kvw, BLK), BF16)
+
+        @pl.when(has_prev)
+        def _():
+            k_dn.wait_send()
+            v_dn.wait_send()
+            k_up.wait_recv()
+            v_up.wait_recv()
+
+        @pl.when(jnp.logical_not(has_prev))
+        def _():
+            kn[pl.ds(0, BLK), :] = jnp.zeros((BLK, kvw), BF16)
+            vt[:, pl.ds(0, BLK)] = jnp.zeros((kvw, BLK), BF16)
 
     key_w = 3 * BLK
     ones = jnp.ones((16, key_w), BF16)
     sinks = sink[...] * LOG2E
     pairs = qw // HEAD // 2
 
-    def attend_chunk(i, hosted):
-        todo = [(i * per + u, p) for u in range(per) for p in range(pairs)]
-        los = {}
-
-        def scores(n):
-            b, p = todo[n]
-            return mm(kn[b * BLK : b * BLK + key_w, :], qt[b, :, 2 * p * BLK : 2 * (p + 1) * BLK])
-
-        def weigh(n, s_all):
-            b, p = todo[n]
+    def attend_pair(b, p):
+        def run():
+            s_all = mm(kn[b * BLK : b * BLK + key_w, :], qt[b, :, 2 * p * BLK : 2 * (p + 1) * BLK])
+            yield
             lo, hi = bias_m[0], bias_m[1]
             if b == 0:
                 lo = lo + jnp.where(idx == 0, NEG, 0.0)
@@ -587,13 +636,11 @@
                 m = jnp.maximum(jnp.max(s, axis=0, keepdims=True), sk)
                 probs.append(jnp.exp2(s - m).astype(BF16))
                 adds.append(jnp.exp2(sk - m))
-            return jnp.concatenate(probs, axis=1), adds
-
-        def value(n, probs, adds):
-            b, p = todo[n]
+            yield
             g = 2 * p // q_per
             vals = jnp.concatenate([vt[g * HEAD : (g + 1) * HEAD, b * BLK : b * BLK + key_w], ones], axis=0)
-            o = mm(vals, probs)
+            o = mm(vals, jnp.concatenate(probs, axis=1))
+            yield
             outs = []
             for u in range(2):
                 cols = slice(u * BLK, (u + 1) * BLK)
@@ -602,33 +649,82 @@
             z[b * BLK : (b + 1) * BLK, p * LANE : (p + 1) * LANE] = (
                 jnp.concatenate(outs, axis=0).T.astype(BF16)
             )
-
-        state = {0: scores(0)}
-
-        def step(n):
-            def run():
-                if n + 1 < len(todo):
-                    state[n + 1] = scores(n + 1)
-                state[n] = weigh(n, state[n])
-            return run
-
-        def close(n):
-            return lambda: value(n, *state.pop(n))
-
-        done = 0
-        for n in range(len(todo)):
-            step(n)()
-            want = ((n + 1) * len(hosted)) // len(todo)
-            while done < want:
-                hosted[done]()
-                done += 1
-            close(n)()
-
-    for i in range(nchunk):
-        maybe_hop(i)
-        with jax.named_scope("attend"):
-            attend_chunk(i, (q_units(i + 1) if i + 1 < nchunk else []) + gate_units(i))
+        return run
+
+    seq = []
+    for n, i in enumerate(visit):
+        if n > 0:
+            seq.append(action(functools.partial(maybe_hop, n)))
+        if i == 0:
+            seq.append(action(kv_halo))
+        todo = [attend_pair(i * per + u, p) for u in range(per) for p in range(pairs)]
+        hosted = q_units(visit[n + 1]) if n + 1 < nchunk else []
+        seq += blend(todo[:-3], hosted) + todo[-3:]
+    with jax.named_scope("attend"):
+        pipeline(seq)
     maybe_hop(nchunk)
+
+    envs = {}
+
+    def mix_begin(b):
+        def run():
+            env = envs[b] = {}
+            c = ct[b]
+            step = st[b]
+            e = c - jnp.log2(jnp.maximum(step, 1e-37))
+            cols = [v.astype(F32) for v in pieces(e)] + [jnp.ones((3 * hd2, LANE), F32)]
+            cols += [jnp.zeros((LANE - 6 * hd2, LANE), F32)]
+            env["lhs"] = jnp.concatenate(cols, axis=0).T.astype(BF16)
+            env["c"] = [v.astype(F32) for v in pieces(c)]
+            env["both"] = jnp.log2(jnp.maximum(step[0:heads] + step[heads:], 1e-37))
+            rows = slice(b * BLK, (b + 1) * BLK)
+            for g in range(groups):
+                bm = bc[rows, g * STATE : (g + 1) * STATE]
+                cm = bc[rows, state_w + g * STATE : state_w + (g + 1) * STATE]
+                env[g] = mm_t(bm, cm)
+        return run
+
+    hrow = lax.broadcasted_iota(jnp.int32, (hd2, BLK), 0)
+
+    def mix_diff(b, h):
+        def run():
+            env = envs[b]
+            parts = []
+            for r in (h, heads + h):
+                own = hrow == r
+                minus = jnp.where(own, -1.0, 0.0).astype(F32)
+                rhs = [minus] * 3 + [jnp.where(own, v, 0.0) for v in env["c"]]
+                rhs += [jnp.zeros((LANE - 6 * hd2, BLK), F32)]
+                parts.append(jnp.concatenate(rhs, axis=0).astype(BF16))
+            env["d", h] = mm(env["lhs"], jnp.concatenate(parts, axis=1))
+        return run
+
+    def mix_head(b, h):
+        def run():
+            env = envs[b]
+            d = env.pop(("d", h))
+            arg = jnp.where(ri < ci, d[:, 0:BLK], d[:, BLK:])
+            arg = jnp.where(ri == ci, spread(env["both"], h, BLK), arg)
+            weights = (env[h // per_group] * jnp.exp2(arg)).astype(BF16)
+            yield
+            y = mm(xt[b, h * HEAD : (h + 1) * HEAD, :], weights)
+            yield
+            ys[b, h * HEAD : (h + 1) * HEAD, :] = y
+        return run
+
+    heads_of = [(b, h) for b in range(nb) for h in range(heads)]
+    ahead = 2
+    seq = [mix_begin(0)] + [mix_diff(*heads_of[n]) for n in range(ahead)]
+    todo = []
+    for n, (b, h) in enumerate(heads_of):
+        if h == heads // 2 and b + 1 < nb:
+            todo.append(mix_begin(b + 1))
+        if n + ahead < len(heads_of):
+            todo.append(mix_diff(*heads_of[n + ahead]))
+        todo.append(mix_head(b, h))
+    seq += blend(todo, [u for i in range(nchunk) for u in gate_units(i)])
+    with jax.named_scope("mix1"):
+        pipeline(seq)
 
     with jax.named_scope("w_chain"):
         for d in range(2):
@@ -652,83 +748,53 @@
                 if b != order[-1]:
                     total = total * spread(dec[b], d * heads + h, HEAD) + gs[b, d, rows, :]
 
-    attn_w = qw
-    zero_pad = jnp.zeros((LANE - hd2, LANE), F32)
-
-    def mix_steps(b):
-        rows = pl.ds(pl.multiple_of(b * BLK, BLK), BLK)
-        env = {}
-
-        def begin():
-            c = ct[b]
-            step = st[b]
-            e = c - jnp.log2(jnp.maximum(step, 1e-37))
-            env["c"] = c
-            env["en"] = jnp.concatenate([e, zero_pad], axis=0).T
-            env["both"] = jnp.log2(jnp.maximum(step[0:heads] + step[heads:], 1e-37))
-            env["grow"] = jnp.exp2(c)
-
-        def open_group(g):
-            def run():
-                bm = bc[rows, g * STATE : (g + 1) * STATE]
-                cm = bc[rows, state_w + g * STATE : state_w + (g + 1) * STATE]
-                env["scores"] = mm_t(bm, cm)
-                states = jnp.concatenate(
-                    [sb[b, d, g * gwid : (g + 1) * gwid, :] for d in range(2)], axis=0
-                )
-                env["carried"] = mm_t(states, cm)
-                env["gated"] = []
-            return run
-
-        def head(g, u):
-            def run():
+    def mix_close(k, u, g):
+        b = chunk_base(k) // BLK + u
+        part = slice(u * BLK, (u + 1) * BLK)
+
+        def run():
+            rows = pl.ds(pl.multiple_of(b * BLK, BLK), BLK)
+            cm = bc[rows, state_w + g * STATE : state_w + (g + 1) * STATE]
+            states = jnp.concatenate(
+                [sb[b, d, g * gwid : (g + 1) * gwid, :] for d in range(2)], axis=0
+            )
+            carried = mm_t(states, cm)
+            yield
+            grow = jnp.exp2(ct[b])
+            gated = []
+            for u in range(per_group):
                 h = g * per_group + u
-                c, en, carried, grow = env["c"], env["en"], env["carried"], env["grow"]
-                arg = jnp.where(
-                    ri < ci,
-                    spread(c, h, BLK) - jnp.broadcast_to(en[:, h : h + 1], sq),
-                    spread(c, heads + h, BLK) - jnp.broadcast_to(en[:, heads + h : heads + h + 1], sq),
-                )
-                arg = jnp.where(ri == ci, spread(env["both"], h, BLK), arg)
-                weights = (env["scores"] * jnp.exp2(arg)).astype(BF16)
-                y = mm(xt[b, h * HEAD : (h + 1) * HEAD, :], weights)
+                y = ys[b, h * HEAD : (h + 1) * HEAD, :]
                 y = y + carried[u * HEAD : (u + 1) * HEAD] * spread(grow, h, HEAD)
                 y = y + carried[gwid + u * HEAD : gwid + (u + 1) * HEAD] * spread(grow, heads + h, HEAD)
-                env["gated"].append(y * gt[b, h * HEAD : (h + 1) * HEAD, :])
-            return run
-
-        def close_group(g):
-            def run():
-                gated = env["gated"]
-                total = sum(jnp.sum(v * v, axis=0, keepdims=True) for v in gated)
-                inv = lax.rsqrt(total * (1.0 / gwid) + epsilon)
-                for t in range(per_group // 2):
-                    s = g * gwid + t * LANE
-                    v = jnp.concatenate([gated[2 * t], gated[2 * t + 1]], axis=0)
-                    z[rows, attn_w + s : attn_w + s + LANE] = (v * inv * ggt[s : s + LANE, :]).T.astype(BF16)
-            return run
-
-        steps = [begin]
-        for g in range(groups):
-            steps.append(open_group(g))
-            steps += [head(g, u) for u in range(per_group)]
-            steps.append(close_group(g))
-        return steps
+                gated.append(y * gt[b, h * HEAD : (h + 1) * HEAD, :])
+            total = sum(jnp.sum(v * v, axis=0, keepdims=True) for v in gated)
+            inv = lax.rsqrt(total * (1.0 / gwid) + epsilon)
+            for t in range(per_group // 2):
+                s = g * gwid + t * LANE
+                v = jnp.concatenate([gated[2 * t], gated[2 * t + 1]], axis=0)
+                zs[k][part, s : s + LANE] = (v * inv * ggt[s : s + LANE, :]).T.astype(BF16)
+        return run
 
     for c in oc[:2]:
         c.wait()
     half_rows = T // 2
     steps = half_rows // ROWS
     width = wo.shape[1]
+    cut = 2
+    wide = width // cut
     copies = [
-        pltpu.make_async_remote_copy(
-            src_ref=psend.at[pl.ds(i * ROWS, ROWS)],
-            dst_ref=precv.at[pl.ds(i * ROWS, ROWS)],
-            send_sem=sem_ps.at[i],
-            recv_sem=sem_pr.at[i],
-            device_id={"tp": peer},
-            device_id_type=MESH,
-        )
+        [
+            pltpu.make_async_remote_copy(
+                src_ref=psend.at[pl.ds(i * ROWS, ROWS), pl.ds(j * wide, wide)],
+                dst_ref=precv.at[pl.ds(i * ROWS, ROWS), pl.ds(j * wide, wide)],
+                send_sem=sem_ps.at[cut * i + j],
+                recv_sem=sem_pr.at[cut * i + j],
+                device_id={"tp": peer},
+                device_id_type=MESH,
+            )
+            for j in range(cut)
+        ]
         for i in range(steps)
     ]
 
@@ -743,7 +809,8 @@
 
         def unit(s):
             def run():
-                part = mm(z[zr, :], wo[:, s : s + 256])
+                part = mm(jnp.concatenate([z[zr, :], zs[k][...]], axis=1), wo[:, s : s + 256])
+                yield
                 if k < steps:
                     psend[dst, s : s + 256] = part.astype(BF16)
                 else:
@@ -755,23 +822,26 @@
         return [unit(s) for s in range(0, width, 256)]
 
     total_chunks = 2 * steps
+    seq = []
     for k in range(total_chunks + 1):
-        if k > steps:
-            with jax.named_scope("w_p"):
-                copies[k - 1 - steps].wait()
-        with jax.named_scope("mix"):
-            hosted = out_units(k - 1) if k > 0 else []
-            main = []
-            if k < total_chunks:
-                for u in range(per):
-                    main += mix_steps(chunk_base(k) // BLK + u)
-            if main:
-                interleave(main, hosted)
-            else:
-                for piece in hosted:
-                    piece()
-        if 0 < k <= steps:
-            copies[k - 1].start()
+        hosted = out_units(k - 1) if k > 0 else []
+        main = []
+        if k < total_chunks:
+            for u in range(per):
+                for g in range(groups):
+                    main.append(mix_close(k, u, g))
+        apart = len(hosted) // cut
+        units = list(hosted)
+        for j in range(cut - 1, -1, -1):
+            if k > steps:
+                units.insert(j * apart, action(copies[k - 1 - steps][j].wait))
+            elif k > 0 and j > 0:
+                units.insert(j * apart + 1, action(copies[k - 1][j - 1].start))
+        if 1 < k <= steps + 1:
+            units.insert(2 if k > steps else 1, action(copies[k - 2][cut - 1].start))
+        seq += blend(units, main) if units else main
+    with jax.named_scope("mix2"):
+        pipeline(seq)
 
 
 def tables(tokens, count):
@@ -826,7 +896,7 @@
         V((depth, wcols), BF16), V((LANE, depth), BF16),
         V((w_out_attn.shape[0] + w_out_state.shape[0], width), BF16),
         V((2, inner_w, STATE), F32),
-        V((T, half), BF16), V((T, half), BF16), V((T, 2 * half), BF16), V((T, LANE), F32),
+        V((T, half), BF16), V((T, half), BF16), V((T, half), BF16), V((T, half), BF16), V((T, LANE), F32),
         V((2, nb, 2 * HEAD, LANE), F32),
         V((T + 2 * BLK, kvw), BF16), V((kvw, T + 2 * BLK), BF16),
         V((xw // LANE, T + 2 * EDGE, LANE), F32),
@@ -835,13 +905,13 @@
         V((nb, hd2, BLK), F32), V((nb, hd2, BLK), F32), V((nb, hd2, BLK), F32), V((nb, hd2, BLK), F32),
         V((inner_w, LANE), F32), V((2, BLK, BLK), F32),
         V((nb, 2, inner_w, STATE), F32), V((2, inner_w, STATE), F32), V((hd2, LANE), F32),
-        V((nb, 2, inner_w, STATE), BF16),
-        V((T, qw + inner_w), BF16),
+        V((nb, 2, inner_w, STATE), BF16), V((nb, inner_w, BLK), F32),
+        V((T, qw), BF16), *[V((ROWS, inner_w), BF16) for _ in range(4)],
         V((T // 2, width), BF16), V((T // 2, width), BF16),
         V((2, xw // LANE, EDGE, LANE), F32),
         V((2, inner_w, STATE), BF16), V((2, inner_w, STATE), BF16),
-        dma((len(small),)), dma((10,)), dma((nchunk,)), dma((nchunk,)), dma((nchunk,)),
-        dma((6,)), dma((6,)), dma((2 * groups,)), dma((2 * groups,)), dma((steps,)), dma((steps,)),
+        dma((len(small),)), dma((17,)), dma((nchunk,)), dma((nchunk,)), dma((nchunk,)),
+        dma((6,)), dma((6,)), dma((2 * groups,)), dma((2 * groups,)), dma((2 * steps,)), dma((2 * steps,)),
     ]
     return pl.pallas_call(
         functools.partial(kernel, n_sp=n_sp),

time: 46.4 us -> 42.6 us (0.918)
  Pallas kernels: 44.9 us -> 41.1 us
    pallas_call x1, Pallas kernels: 44.9 us -> 41.1 us  [local(): pl.pallas_call(functools.partial(kernel, n_sp=n_sp), out_shape=pltpu.VMEM...]
where the time goes in v3:
time: 42.6 us; the launch traced here: 42.4 us
  Pallas kernels  41.1 us (96%)
  local copies, waits for them, and re-layouts  1.32 us (3%)
    pallas_call x1, Pallas kernels, local(): pl.pallas_call(functools.partial(kernel, n_sp=n_sp), out_shape=pltpu.VMEM...  41.1 us
    unnamed x1, local copies, waits for them, and re-layouts  1.32 us

profile of v3, /device:TPU:0, one launch (start us, length us, event | category | flops | bytes accessed | tf_op | source)
XLA Modules:
  0.0 42.4 jit_solution(12970278853472495291)
XLA Ops:
  0.0 41.1 %mixer.1 = bf16[512,2048]{1,0:T(8,128)(2,1)S(1)} custom-call(bf16[1024,1024]{1,0:T(8,128)(2,1)} %x_hbm.1, bf16[2048,512]{1,0:T(8,128)(2,1)} %wq.1, bf16[2048,128]{1,0:T(8,128)(2,1)} %wk.1, bf16[2048,128]{1,0:T(8,128)(2,1)} %wv.1, bf16[2048,512]{1,0:T(8,128)(2,1)} %wi.1, bf16[2048,256]{1,0:T(8,128)(2,1)} %wb.1, bf16[2048,256]{1,0:T(8,128)(2,1)} %wc.1, ...), custom_call_target="tpu_custom_call" | custom-call | tf_op jit(solution)/shard_map/mixer/pallas_call | solution.py:916
  41.1 1.3 %copy.30 = bf16[512,2048]{1,0:T(8,128)(2,1)} copy(bf16[512,2048]{1,0:T(8,128)(2,1)S(1)} %mixer.1) | data formatting | bytes 4194304
